TPU v7x, 128 devices: a whole 4x4x4 slice. The times are simulated.
128 devices in a mesh: sp: 16 (over z, x), tp: 8 (over y, core).
Axes of the slice: x: 4, y: 4, z: 4, core: 2. Of those that a mesh axis runs over, the one named last changes fastest.
Arguments:
- queries: bfloat16 [16384, 1024], P('sp', 'tp'), may hold values from -6 to 6, as said below
- key_rows: bfloat16 [16384, 1024], P('sp', 'tp'), may hold values from -6 to 6, as said below
- value_rows: bfloat16 [16384, 1024], P('sp', 'tp'), may hold values from -6 to 6
- lambdas: float32 [8], P('tp'), may hold values from 0.3 to 0.8
- head_gain: float32 [128], replicated, may hold values from 0.1 to 1.9
- out_weight: bfloat16 [1024, 2048], replicated, may hold values from -0.1875 to 0.1875
- stream: bfloat16 [16384, 2048], P(('sp', 'tp')), may hold values from -6 to 6
- ffn_gain: float32 [2048], replicated, may hold values from 0.1 to 1.9
- routes: int32 [16384, 2], P(('sp', 'tp')), may hold values from 0 to 15, all different within a row; in each aligned block of 128 rows (0 to 127, 128 to 255, ...) at most 20 rows name the same one
- route_weight: float32 [16384, 2], P(('sp', 'tp')), may hold values from 0.1 to 1
- gate_weight: bfloat16 [16, 2048, 5120], P('sp', None, 'tp'), may hold values from -0.125 to 0.125
- up_weight: bfloat16 [16, 2048, 5120], P('sp', None, 'tp'), may hold values from -0.125 to 0.125
- down_weight: bfloat16 [16, 5120, 2048], P('sp', 'tp'), may hold values from -0.078125 to 0.078125
Outputs:
- layer_out: bfloat16 [16384, 2048], P(('sp', 'tp'))
Inputs may be any that keep to these rules, and one draw needn't show every extreme that they name: Custom draw; the queries of a position meet only keys of the same or earlier positions. `key_rows`: custom draw. `routes`: each row names 2 different experts. In the 128 rows of one device no expert is named by more than 20 rows, and every draw reaches 20 on some device.
All inputs are finite; a program needn't handle non-finite values.
Results may differ from a plain program's by a relative error of at most 0.01.
Values may be sent and summed in bfloat16 or wider, within the bound.
No kernel may reach another device: no remote copies, remote signals or barrier semaphores. Data moves between devices by JAX's collectives and lax.ppermute only.
A program may use at most 128 MiB of HBM per device.

v0:
```python
import math

import jax
import jax.numpy as jnp
from jax import lax
from jax.experimental import pallas as pl
from jax.experimental.pallas import tpu as pltpu
from jax.sharding import PartitionSpec as P


DH = 64
PIECE = 512
ROWS = 256
SCALE = DH**-0.5 * math.log2(math.e)
BOTH = ("sp", "tp")
F32 = jnp.float32
BF16 = jnp.bfloat16
VMEM_LIMIT = 58 * 1024 * 1024
ATTENTION_LIMIT = 26 * 1024 * 1024
CHUNKS = 2
CUTS = 4
SHARERS = 2
FLOPS_US = 1.0e9


def dot(a, b, dims=((1,), (0,))):
    return lax.dot_general(a, b, (dims, ((), ())), preferred_element_type=F32)


def attention_body(pieces, side, first, final, count, *refs):
    sp_ref, lam_ref, gain_ref, q_ref = refs[:4]
    kv_refs, refs = refs[4 : 4 + count], refs[4 + count :]
    if first:
        m_ref, acc_ref = None, None
    else:
        (m_ref, acc_ref), refs = refs[:2], refs[2:]
    if final:
        (o_ref, m_sc, acc_sc), refs = refs[:3], refs[3:]
    else:
        (m_sc, acc_sc), refs = refs[:2], refs[2:]
    kv, sem, order, base_at, bounds = refs[:5]
    sp = sp_ref[0]
    z, x = sp // side, sp % side
    blocks = side * side
    begin = 0
    copies = []
    for n, ref in enumerate(kv_refs):
        copies.append(pltpu.make_async_copy(ref, kv.at[pl.ds(begin, ref.shape[0])], sem.at[n]))
        begin += ref.shape[0]
    for c in copies:
        c.start()
    if first:
        m_sc[...] = jnp.full(m_sc.shape, -1e30, F32)
        acc_sc[...] = jnp.zeros(acc_sc.shape, F32)
    else:
        m_sc[...] = m_ref[...]
        acc_sc[...] = acc_ref[...]

    mine = (blocks - 1 - sp, sp)
    for n, (dz, dx, low) in enumerate(pieces):
        block = (z + dz + side) % side * side + (x + dx + side) % side
        base_at[n] = block * (2 * PIECE) + low * PIECE
        for h in range(2):
            spot = jnp.int32(0) if n == 0 else bounds[h]
            order[h, spot] = jnp.int32(n)
            bounds[h] = spot + (block < mine[h]).astype(jnp.int32)
    for h in range(2):
        spot = bounds[h]
        for n in range(len(pieces)):
            order[h, spot] = jnp.int32(n)
            spot = spot + (base_at[n] // (2 * PIECE) == mine[h]).astype(jnp.int32)
        bounds[2 + h] = spot
    for c in copies:
        c.wait()

    rows = q_ref.shape[2]

    def step(h, at, masked):
        keys = len(at) * PIECE

        def operands():
            parts = [kv[pl.ds(pl.multiple_of(p * PIECE, PIECE), PIECE), :] for p in at]
            v = jnp.concatenate([p[:, 128:] for p in parts], axis=0)
            return (
                jnp.concatenate([p[:, :128] for p in parts], axis=0),
                jnp.concatenate([v, jnp.ones((keys, 128), BF16)], axis=1),
            )

        def tile(r):
            return pl.ds(r * ROWS if isinstance(r, int) else pl.multiple_of(r * ROWS, ROWS), ROWS)

        def scores(m, r, k):
            s = dot(q_ref[h, m, tile(r), :], k, ((1,), (1,)))
            if masked:
                row = r * ROWS + lax.broadcasted_iota(jnp.int32, s.shape, 0)
                start = jnp.where(h == 0, (blocks - 1 - sp) * (2 * PIECE) + 64, sp * (2 * PIECE))
                q_at = start + lax.shift_right_logical(row, 6) * 128 + (row & 63)
                key = lax.broadcasted_iota(jnp.int32, s.shape, 1)
                key = key + jnp.where(key < PIECE, base_at[at[0]], base_at[at[-1]] - (keys - PIECE))
                s = jnp.where(key <= q_at, s, -1e30)
            return s

        def finish(m, r, s, v):
            to = tile(r)
            old = m_sc[h, m, to, :]
            new = jnp.maximum(old, jnp.max(s, axis=1, keepdims=True))
            m_sc[h, m, to, :] = new
            p = jnp.exp2((s - jnp.concatenate([new] * (keys // 128), axis=1)) * SCALE)
            factor = jnp.exp2((old - new) * SCALE)
            both = jnp.concatenate([factor, factor], axis=1)
            acc_sc[h, m, to, :] = acc_sc[h, m, to, :] * both + dot(p.astype(BF16), v)

        def run(tiles):
            k, v = operands()
            s = scores(*tiles[0], k)
            for n, at_tile in enumerate(tiles):
                after = scores(*tiles[n + 1], k) if n + 1 < len(tiles) else None
                finish(*at_tile, s, v)
                s = after

        if len(at) == 2 and not masked:
            run([(m, r) for r in range(rows // ROWS) for m in range(2)])
        else:

            def some(r, carry):
                run([(m, r) for m in range(2)])
                return carry

            lax.fori_loop(0, rows // ROWS, some, 0)

    def half(h, carry):
        number = bounds[h]

        def pair(n, inner):
            step(h, (order[h, 2 * n], order[h, 2 * n + 1]), False)
            return inner

        lax.fori_loop(0, number // 2, pair, 0)

        @pl.when(number % 2 == 1)
        def _():
            step(h, (order[h, number - 1],), False)

        if not final:

            @pl.when(bounds[2 + h] > number)
            def _():
                step(h, (order[h, number], order[h, number + 1]), True)

        return carry

    lax.fori_loop(0, 2, half, 0)
    if final:
        def close(h, carry):
            c0 = acc_sc[h, 0, :, :128] / acc_sc[h, 0, :, 128:]
            c1 = acc_sc[h, 1, :, :128] / acc_sc[h, 1, :, 128:]
            c = c0 - lam_ref[0] * c1
            c = c * lax.rsqrt(jnp.mean(c * c, axis=1, keepdims=True) + 1e-05) * gain_ref[...]
            o_ref[jnp.where(sp < blocks // 2, 1 - h, h)] = c.astype(BF16)
            return carry

        lax.fori_loop(0, 2, close, 0)


def attention(q, arrays, pieces, state, lambdas, gain, sp, side, final):
    half = q.shape[2]
    first = state is None
    whole = pl.BlockSpec(memory_space=pltpu.VMEM)
    scalar = pl.BlockSpec(memory_space=pltpu.SMEM)
    held = (
        jax.ShapeDtypeStruct((2, 2, half, 128), F32),
        jax.ShapeDtypeStruct((2, 2, half, 256), F32),
    )
    scratch = [
        pltpu.VMEM((len(pieces) * PIECE, arrays[0].shape[1]), BF16),
        pltpu.SemaphoreType.DMA((len(arrays),)),
        pltpu.SMEM((2, len(pieces) + 2), jnp.int32),
        pltpu.SMEM((len(pieces),), jnp.int32),
        pltpu.SMEM((4,), jnp.int32),
    ]
    if final:
        scratch = [pltpu.VMEM(h.shape, F32) for h in held] + scratch
    return pl.pallas_call(
        lambda *refs: attention_body(pieces, side, first, final, len(arrays), *refs),
        in_specs=[scalar, scalar, whole, whole]
        + [pl.BlockSpec(memory_space=pl.ANY)] * len(arrays)
        + ([] if first else [whole, whole]),
        out_specs=whole if final else (whole, whole),
        out_shape=jax.ShapeDtypeStruct((2, half, 128), BF16) if final else held,
        scratch_shapes=scratch,
        compiler_params=pltpu.CompilerParams(vmem_limit_bytes=ATTENTION_LIMIT),
        cost_estimate=cost(len(pieces)),
        name="attention",
    )(sp.reshape(1), lambdas, gain.reshape(1, 128), q, *arrays, *(() if first else state))


def spread(array, forth, back):
    half = array.shape[0] // 2
    before, behind = lax.ppermute(array, "sp", forth), lax.ppermute(array, "sp", back)
    far = lax.ppermute(before[:half], "sp", forth), lax.ppermute(behind[half:], "sp", back)
    return (before, behind), far


def attend(queries, key_rows, value_rows, lambdas, head_gain, weights, swap):
    sp_size, tp_size = lax.axis_size("sp"), lax.axis_size("tp")
    side = math.isqrt(sp_size)
    sp = lax.axis_index("sp")
    length = queries.shape[0]
    kv = jnp.concatenate([key_rows, value_rows], axis=1)
    ring = {}
    for name, dz, dx in (("z+", 1, 0), ("z-", -1, 0), ("x+", 0, 1), ("x-", 0, -1)):
        ring[name] = [
            (s, (s // side + dz) % side * side + (s % side + dx) % side) for s in range(sp_size)
        ]
    along_z, along_x = (ring["z+"], ring["z-"]), (ring["x+"], ring["x-"])
    upper, lower = kv[: length // 2], kv[length // 2 :]
    split = queries.reshape(tp_size, 2, length // (2 * tp_size), queries.shape[1])
    own = split[:, 0].reshape(length // 2, -1)
    near_u, far_u = spread(upper, *along_x)
    near_l, far_l = spread(lower, *along_z)
    other = lax.ppermute(
        split[:, 1].reshape(length // 2, -1), "sp", [(s, sp_size - 1 - s) for s in range(sp_size)]
    )
    row = jnp.concatenate([upper, *near_u, *far_u], axis=0)
    column = jnp.concatenate([lower, *near_l, *far_l], axis=0)
    near_row, far_row = spread(row, *along_z)
    near_column, far_column = spread(column, *along_x)
    steps = (0, -1, 1, 2)

    zero = jnp.zeros((2, length // 2, DH), BF16)
    q = jnp.stack([other, own])
    q = jnp.stack(
        [jnp.concatenate([q[..., :DH], zero], -1), jnp.concatenate([zero, q[..., DH:]], -1)], 1
    )
    calls = (
        ((row, column), [(0, d, 0) for d in steps] + [(d, 0, 1) for d in steps]),
        (
            near_row + near_column,
            [(e, d, 0) for e in (-1, 1) for d in steps] + [(d, e, 1) for e in (-1, 1) for d in steps],
        ),
        (far_row + far_column, [(2, d, 0) for d in steps] + [(d, 2, 1) for d in steps]),
    )
    state = None
    for n, (arrays, pieces) in enumerate(calls):
        state = attention(
            q, arrays, pieces, state, lambdas, head_gain, sp, side, n + 1 == len(calls)
        )
        if n == 0:
            weights, state = lax.optimization_barrier((weights, state))
            swapped = tuple(swap(w) for w in weights)
    return state, swapped


def project_body(h_ref, w_ref, s_ref, g_ref, d_ref, a_ref, *o_refs):
    parts = [jnp.concatenate([h_ref[n, t] for t in range(h_ref.shape[1])], axis=1) for n in range(2)]
    x = jnp.concatenate(parts, axis=0)
    attended = s_ref[...].astype(F32) + dot(x, w_ref[...])
    a_ref[...] = attended
    mean = jnp.mean(attended * attended, axis=1, keepdims=True)
    normed = (attended * lax.rsqrt(mean + 1e-06) * g_ref[...]).astype(BF16)
    pieces = stacked(normed)
    for c, o_ref in enumerate(o_refs):
        rows = dot(d_ref[c], pieces).astype(BF16)
        for h in range(SHARERS):
            o_ref[h] = rows


def stacked(x):
    wide = x.shape[1] // CUTS
    return jnp.concatenate([x[:, n * wide : (n + 1) * wide] for n in range(CUTS)], axis=0)


def project(heads, out_weight, stream, gain, dispatch):
    rows, width = stream.shape
    packed = jax.ShapeDtypeStruct((SHARERS, dispatch.shape[1], width // CUTS), BF16)
    return pl.pallas_call(
        project_body,
        out_shape=(jax.ShapeDtypeStruct((rows, width), F32),) + (packed,) * CHUNKS,
        compiler_params=pltpu.CompilerParams(vmem_limit_bytes=VMEM_LIMIT),
        cost_estimate=cost(5),
        name="project",
    )(heads, out_weight, stream, gain.reshape(1, width), dispatch)


def cost(microseconds):
    return pl.CostEstimate(flops=int(microseconds * FLOPS_US), bytes_accessed=0, transcendentals=0)


def expert_body(sets, r_any, s_any, p_any, *refs):
    weights = refs[: 3 * sets]
    o_ref, r_ref, s_ref, p_ref, x_sc, act_sc, acc_sc, in_buf, down_buf, sem, small = refs[3 * sets :]
    hidden = in_buf.shape[2] // 2
    rows = s_ref.shape[0] // CUTS

    def copy(n, kind):
        if kind < 2:
            to = in_buf.at[n, :, pl.ds(kind * hidden, hidden)]
        else:
            to = down_buf.at[n // 2, pl.ds(n % 2 * hidden, hidden), :]
        return pltpu.make_async_copy(weights[3 * n + kind], to, sem.at[3 * n + kind])

    def share(h):
        return pl.ds(pl.multiple_of(h * rows, 16), rows)

    def landed(kind, n):
        if kind < 2:
            to = in_buf.at[n, :, pl.ds(kind * hidden, hidden)]
        else:
            to = down_buf.at[n // 2, pl.ds(pl.multiple_of(n % 2 * hidden, 128), hidden), :]
        pltpu.make_async_copy(weights[kind], to, sem.at[3 * n + kind]).wait()

    first = pltpu.make_async_copy(r_any, r_ref, small.at[0])
    second = pltpu.make_async_copy(s_any, s_ref, small.at[1])
    third = pltpu.make_async_copy(p_any, p_ref, small.at[2])
    order = [
        (2 * p + n, kind)
        for p in range(sets // 2)
        for n, kind in ((0, 0), (0, 1), (1, 0), (1, 1), (0, 2), (1, 2))
    ]
    first.start()
    second.start()
    for n, kind in order[:2]:
        copy(n, kind).start()
    first.wait()
    second.wait()
    for n, kind in order[2:]:
        copy(n, kind).start()
    third.start()
    wide = r_ref.shape[2]

    def unpack(h, carry):
        cuts = dot(s_ref[...], r_ref[h]).astype(BF16)
        for n in range(CUTS):
            x_sc[share(h), n * wide : (n + 1) * wide] = cuts[n * rows : (n + 1) * rows]
        return carry

    lax.fori_loop(0, SHARERS, unpack, 0)

    def pair(p, carry):
        def one(v, inner):
            n = 2 * p + v
            for kind in range(2):
                landed(kind, n)
            both = dot(x_sc[...], in_buf[n])
            gate, upper = both[:, :hidden], both[:, hidden:]
            act = (gate / (1.0 + jnp.exp(-gate)) * upper).astype(BF16)
            act_sc[:, pl.ds(pl.multiple_of(v * hidden, 128), hidden)] = act
            return inner

        lax.fori_loop(0, 2, one, 0)
        landed(2, 2 * p)
        landed(2, 2 * p + 1)
        acc_sc[...] += dot(act_sc[...], down_buf[p])
        return carry

    acc_sc[...] = jnp.zeros(acc_sc.shape, F32)
    lax.fori_loop(0, sets // 2, pair, 0)
    third.wait()

    def repack(h, carry):
        o_ref[h] = dot(p_ref[...], stacked(acc_sc[share(h), :].astype(BF16))).astype(BF16)
        return carry

    lax.fori_loop(0, SHARERS, repack, 0)


def expert(arrived, select, place, sets):
    rows = SHARERS * select.shape[0] // CUTS
    width, hidden = sets[0][0].shape
    flat = [w for one in sets for w in one]
    return pl.pallas_call(
        lambda *refs: expert_body(len(sets), *refs),
        in_specs=[pl.BlockSpec(memory_space=pl.ANY)] * (3 + len(flat)),
        out_specs=pl.BlockSpec(memory_space=pltpu.VMEM),
        out_shape=jax.ShapeDtypeStruct(arrived.shape, BF16),
        scratch_shapes=[
            pltpu.VMEM(arrived.shape, BF16),
            pltpu.VMEM(select.shape, BF16),
            pltpu.VMEM(place.shape, BF16),
            pltpu.VMEM((rows, width), BF16),
            pltpu.VMEM((rows, 2 * hidden), BF16),
            pltpu.VMEM((rows, width), F32),
            pltpu.VMEM((len(sets), width, 2 * hidden), BF16),
            pltpu.VMEM((len(sets) // 2, 2 * hidden, width), BF16),
            pltpu.SemaphoreType.DMA((len(flat),)),
            pltpu.SemaphoreType.DMA((3,)),
        ],
        compiler_params=pltpu.CompilerParams(vmem_limit_bytes=VMEM_LIMIT),
        cost_estimate=cost(16),
        name="expert",
    )(arrived, select, place, *flat)


def combine_body(*refs):
    r_refs, (w_ref, a_ref, o_ref, r_sc) = refs[:CHUNKS], refs[CHUNKS:]
    wide = r_refs[0].shape[2]
    rows = a_ref.shape[0]
    for c, r_ref in enumerate(r_refs):
        total = sum(r_ref[h].astype(F32) for h in range(SHARERS))
        r_sc[c * total.shape[0] : (c + 1) * total.shape[0], :] = total.astype(BF16)

    def one(n, carry):
        at = pl.ds(pl.multiple_of(n * wide, 128), wide)
        both = dot(w_ref[n], r_sc[...])
        o_ref[:, at] = (a_ref[:, at] + (both[:rows] + both[rows:])).astype(BF16)
        return carry

    lax.fori_loop(0, CUTS, one, 0)


def combine(returned, weights, attended):
    return pl.pallas_call(
        combine_body,
        out_shape=jax.ShapeDtypeStruct(attended.shape, BF16),
        scratch_shapes=[pltpu.VMEM((weights.shape[2], attended.shape[1] // CUTS), BF16)],
        compiler_params=pltpu.CompilerParams(vmem_limit_bytes=VMEM_LIMIT),
        name="combine",
    )(*returned, weights, attended)


def moved(sp_size, tp_size, shift, flip):
    pairs = []
    for s in range(sp_size):
        for t in range(tp_size):
            y, c = t // 2, t % 2
            to = (y + shift(c)) % (tp_size // 2) * 2 + (c ^ flip)
            pairs.append((s * tp_size + t, s * tp_size + to))
    return pairs


def local(
    queries,
    key_rows,
    value_rows,
    lambdas,
    head_gain,
    out_weight,
    stream,
    ffn_gain,
    routes,
    route_weight,
    gate_weight,
    up_weight,
    down_weight,
):
    sp_size = lax.axis_size("sp")
    tp_size = lax.axis_size("tp")
    sp = lax.axis_index("sp")
    rows_local, width = stream.shape
    experts = sp_size * gate_weight.shape[0]
    top_count = routes.shape[1]
    low = sp < sp_size // 2

    mine = (gate_weight[0], up_weight[0], down_weight[0])
    along = moved(sp_size, tp_size, lambda c: 2 * c - 1, 0)
    sibling = moved(sp_size, tp_size, lambda c: 0, 1)
    passed = []
    for w in mine:
        passed.append(lax.ppermute(w, BOTH, along))
    passed = tuple(passed)

    slots = max(2, (rows_local * top_count * 5 + 4 * experts - 1) // (4 * experts))
    part = slots // CHUNKS
    flat = routes.reshape(-1)
    onehot = (flat[:, None] == jnp.arange(experts, dtype=jnp.int32)[None, :]).astype(BF16)
    count = flat.shape[0]
    earlier = (jnp.arange(count)[None, :] < jnp.arange(count)[:, None]).astype(BF16)
    slot = jnp.sum(dot(earlier, onehot) * onehot.astype(F32), axis=1).astype(jnp.int32)
    packed = experts * part * CUTS
    places = jnp.arange(packed, dtype=jnp.int32)

    def spots(k):
        e, j = (v.reshape(rows_local, top_count)[:, k] for v in (flat, slot))
        return [
            [jnp.where(j // part == c, (e * CUTS + n) * part + j % part, -1) for n in range(CUTS)]
            for c in range(CHUNKS)
        ]

    chosen = [spots(k) for k in range(top_count)]
    dispatch = sum(
        (places[:, None] == jnp.stack([jnp.concatenate(c) for c in at])[:, None, :]).astype(BF16)
        for at in chosen
    )
    every = jnp.arange(CHUNKS * packed, dtype=jnp.int32)
    weighted = sum(
        jnp.where(
            every
            == jnp.stack(
                [
                    sum(jnp.where(at[c][n] < 0, 0, at[c][n] + c * packed) for c in range(CHUNKS))
                    for n in range(CUTS)
                ]
            )[..., None],
            route_weight[:, k : k + 1],
            0.0,
        )
        for k, at in enumerate(chosen)
    )
    weights = jnp.concatenate(
        [weighted.astype(BF16), (weighted - lax.reduce_precision(weighted, 8, 7)).astype(BF16)], axis=1
    )
    row = jnp.arange(experts * part, dtype=jnp.int32)
    cuts = jnp.concatenate([(row // part * CUTS + n) * part + row % part for n in range(CUTS)])
    select = (cuts[:, None] == places).astype(BF16)
    place = (places[:, None] == cuts).astype(BF16)

    heads, mine_too = attend(
        queries, key_rows, value_rows, lambdas, head_gain, mine, lambda w: lax.ppermute(w, BOTH, sibling)
    )
    half = rows_local // 2
    heads = heads.reshape(2 * tp_size, half, 128)
    groups = [
        [s * tp_size + t for s in (n, sp_size - 1 - n) for t in range(tp_size)]
        for n in range(sp_size // 2)
    ]
    heads = lax.all_to_all(
        heads, BOTH, split_axis=0, concat_axis=0, tiled=True, axis_index_groups=groups
    ).reshape(2, tp_size, half, 128)
    heads = jnp.where(low, heads, heads[::-1])

    attended, *outgoing = project(heads, out_weight, stream, ffn_gain, dispatch)

    passed, outgoing = lax.optimization_barrier((passed, outgoing))
    passed_too = tuple(lax.ppermute(w, BOTH, sibling) for w in passed)
    sets = (mine, mine_too, passed, passed_too)

    ring = tp_size // 2
    members = [
        [
            s * tp_size + (y + h * (ring // SHARERS)) * 2 + c
            for h in range(SHARERS)
            for s in range(sp_size)
        ]
        for y in range(ring // SHARERS)
        for c in range(2)
    ]

    def exchange(x):
        x = x.reshape(SHARERS * experts, CUTS * part, width // CUTS)
        return lax.all_to_all(
            x, BOTH, split_axis=0, concat_axis=0, tiled=True, axis_index_groups=members
        ).reshape(SHARERS, packed, width // CUTS)

    arrived = [exchange(x) for x in outgoing]
    returned = [exchange(expert(x, select, place, sets)) for x in arrived]
    return combine(returned, weights, attended)


def solution(mesh):
    placed = (
        P("sp", "tp"),
        P("sp", "tp"),
        P("sp", "tp"),
        P("tp"),
        P(),
        P(),
        P(("sp", "tp"), None),
        P(),
        P(("sp", "tp"), None),
        P(("sp", "tp"), None),
        P("sp", None, "tp"),
        P("sp", None, "tp"),
        P("sp", "tp", None),
    )
    return jax.shard_map(
        local, mesh=mesh, in_specs=placed, out_specs=P(("sp", "tp"), None), check_vma=False
    )
```

profile of v0, /device:TPU:9, one launch (start us, length us, event | category | flops | bytes accessed | tf_op | source)
XLA Modules:
  0.0 249.4 jit_solution(11708617283967556079)
XLA Ops:
  0.0 1.0 constant_dynamic-update-slice_fusion.1
  1.0 1.0 constant_dynamic-update-slice_fusion
  2.1 0.9 fusion.32
  2.9 1.6 collective-permute-start.12
  4.6 2.1 collective-permute-start.13
  6.7 1.2 collective-permute-start.4
  7.9 1.5 collective-permute-start.5
  9.4 2.5 %collective-permute-start.3 = (bf16[512,128]{1,0:T(8,128)(2,1)S(1)}, bf16[512,128]{1,0:T(8,128)(2,1)S(1)}, u32[]{:S(2)}, u32[]{:S(2)}) collective-permute-start(bf16[512,128]{1,0:T(8,128)(2,1)S(1)} %bitcast.199), channel_id=1, source_target_pairs={{0,120},{8,112},{16,104},{24,96},{32,88},{40,80},{48,72},{56,64},{... | collective-permute-start | bytes 393224 | tf_op jit(solution)/shard_map/ppermute | solution.py:221
  13.4 1.4 collective-permute-start
  14.8 0.7 constant_dynamic-update-slice_fusion.10
  15.6 0.7 constant_dynamic-update-slice_fusion.9
  16.4 2.7 %collective-permute-start.15 = (bf16[256,256]{1,0:T(8,128)(2,1)S(1)}, bf16[256,256]{1,0:T(8,128)(2,1)S(1)}, u32[]{:S(2)}, u32[]{:S(2)}) collective-permute-start(bf16[256,256]{1,0:T(8,128)(2,1)S(1)} %slice.93), channel_id=1, source_target_pairs={{0,96},{8,104},{16,112},{24,120},{32,0},{40,8},{48,16},{56,24},{64... | collective-permute-start | bytes 393224 | tf_op jit(solution)/shard_map/ppermute | solution.py:200
  19.0 0.7 constant_dynamic-update-slice_fusion.5
  20.3 0.7 constant_dynamic-update-slice_fusion.4
  21.0 1.0 collective-permute-done.14
  22.0 3.0 %collective-permute-start.7 = (bf16[256,256]{1,0:T(8,128)(2,1)S(1)}, bf16[256,256]{1,0:T(8,128)(2,1)S(1)}, u32[]{:S(2)}, u32[]{:S(2)}) collective-permute-start(bf16[256,256]{1,0:T(8,128)(2,1)S(1)} %slice.88), channel_id=1, source_target_pairs={{0,24},{8,0},{16,8},{24,16},{32,56},{40,32},{48,40},{56,48},{64,88... | collective-permute-start | bytes 393224 | tf_op jit(solution)/shard_map/ppermute | solution.py:200
  25.0 0.7 constant_dynamic-update-slice_fusion.8
  26.4 2.7 %collective-permute-start.18 = (bf16[2048,256]{1,0:T(8,128)(2,1)}, bf16[2048,256]{1,0:T(8,128)(2,1)S(1)}, u32[]{:S(2)}, u32[]{:S(2)}) collective-permute-start(bf16[2048,256]{1,0:T(8,128)(2,1)} %constant_dynamic-update-slice_fusion.7.refs_5_), channel_id=1, source_target_pairs={{0,24},{8,0},{16,8},{24,16},{32,56},{40,32},{48,40},{56,48},{64,88... | collective-permute-start | bytes 3145736 | tf_op jit(solution)/shard_map/ppermute | solution.py:199
  32.3 0.7 pad_add_fusion.1
  33.0 1.5 collective-permute-start.8
  34.5 0.7 maximum_select_fusion
  35.4 16.1 %collective-permute-done.16.refs_6_ = bf16[2048,256]{1,0:T(8,128)(2,1)S(1)} collective-permute-done((bf16[2048,256]{1,0:T(8,128)(2,1)}, bf16[2048,256]{1,0:T(8,128)(2,1)S(1)}, u32[]{:S(2)}, u32[]{:S(2)}) %collective-permute-start.16) | collective-permute-done | bytes 1048608 | tf_op jit(solution)/shard_map/ppermute | solution.py:199
  51.6 2.7 %collective-permute-start.19 = (bf16[1024,256]{1,0:T(8,128)(2,1)S(1)}, bf16[1024,256]{1,0:T(8,128)(2,1)S(1)}, u32[]{:S(2)}, u32[]{:S(2)}) collective-permute-start(bf16[1024,256]{1,0:T(8,128)(2,1)S(1)} %slice.95), channel_id=1, source_target_pairs={{0,24},{8,0},{16,8},{24,16},{32,56},{40,32},{48,40},{56,48},{64,88... | collective-permute-start | bytes 1572872 | tf_op jit(solution)/shard_map/ppermute | solution.py:200
  54.4 0.7 collective-permute-start.11
  55.1 10.1 %attention.3 = (f32[2,2,512,128]{3,2,1,0:T(8,128)S(1)}, f32[2,2,512,256]{3,2,1,0:T(8,128)S(1)}) custom-call(s32[1]{0:T(128)} %bitcast.3.refs_0_, f32[1]{0:T(128)S(6)} %copy.72.refs_1_, f32[1,128]{1,0:T(1,128)S(1)} %bitcast.183, bf16[2,2,512,128]{3,2,1,0:T(8,128)(2,1)S(1)} %pad_maximum_fusion.1.refs_3_, ...), custom_call_target="tpu_custom_call" | custom-call | flops 8000000000 | tf_op jit(solution)/shard_map/attention/pallas_call | solution.py:183
  65.6 4.5 %collective-permute-start.20 = (bf16[2048,640]{1,0:T(8,128)(2,1)}, bf16[2048,640]{1,0:T(8,128)(2,1)}, u32[]{:S(2)}, u32[]{:S(2)}) collective-permute-start(bf16[2048,640]{1,0:T(8,128)(2,1)} %bitcast.refs_3_), channel_id=1, source_target_pairs={{0,1},{1,0},{2,3},{3,2},{4,5},{5,4},{6,7},{7,6},{8,9},{9,8},{10,11... | collective-permute-start | bytes 7864328 | tf_op jit(solution)/shard_map/ppermute | solution.py:508
  70.1 1.8 collective-permute-start.9
  71.9 14.2 %attention.4 = (f32[2,2,512,128]{3,2,1,0:T(8,128)S(1)}, f32[2,2,512,256]{3,2,1,0:T(8,128)S(1)}) custom-call(s32[1]{0:T(128)} %bitcast.3.refs_0_, f32[1]{0:T(128)S(6)} %copy.72.refs_1_, f32[1,128]{1,0:T(1,128)S(1)} %bitcast.184, bf16[2,2,512,128]{3,2,1,0:T(8,128)(2,1)S(1)} %pad_maximum_fusion.1.refs_3_, bf16[2048,256]{1,0:T(8,128)(2,1)S(1)} %collective-permute-done.8.refs_4_, ...), custom_call_target="tpu_custom_call" | custom-call | flops 16000000000 | tf_op jit(solution)/shard_map/attention/pallas_call | solution.py:183
  86.0 8.0 %attention.5 = bf16[2,512,128]{2,1,0:T(8,128)(2,1)} custom-call(s32[1]{0:T(128)} %bitcast.3.refs_0_, f32[1]{0:T(128)S(6)} %copy.72.refs_1_, f32[1,128]{1,0:T(1,128)S(1)} %bitcast.185, bf16[2,2,512,128]{3,2,1,0:T(8,128)(2,1)S(1)} %pad_maximum_fusion.1.refs_3_, bf16[1024,256]{1,0:T(8,128)(2,1)S(1)} %collective-permute-done.9.refs_4_, ...), custom_call_target="tpu_custom_call" | custom-call | flops 8000000000 | tf_op jit(solution)/shard_map/attention/pallas_call | solution.py:183
  94.0 9.3 %all-to-all-start = ((bf16[16,64,128]{2,1,0:T(8,128)(2,1)}), bf16[16,64,128]{2,1,0:T(8,128)(2,1)S(1)}, u32[]{:S(2)}, u32[]{:S(2)}) async-start(bf16[16,64,128]{2,1,0:T(8,128)(2,1)} %bitcast.12), calls=%async_computation | async-start | bytes 524288 | tf_op jit(solution)/shard_map/all_to_all | solution.py:516
  103.3 1.9 fusion.6.d_ref
  105.6 24.7 %all-to-all-done = bf16[16,64,128]{2,1,0:T(8,128)(2,1)S(1)} async-done(((bf16[16,64,128]{2,1,0:T(8,128)(2,1)}), bf16[16,64,128]{2,1,0:T(8,128)(2,1)S(1)}, u32[]{:S(2)}, u32[]{:S(2)}) %all-to-all-start) | async-done | bytes 262176 | tf_op jit(solution)/shard_map/all_to_all | solution.py:516
  130.3 0.8 reverse_select_fusion.h_ref
  131.1 5.7 %project.1 = (f32[128,2048]{1,0:T(8,128)}, bf16[2,640,512]{2,1,0:T(8,128)(2,1)}, bf16[2,640,512]{2,1,0:T(8,128)(2,1)}) custom-call(bf16[2,8,64,128]{3,2,1,0:T(8,128)(2,1)} %reverse_select_fusion.h_ref, bf16[1024,2048]{1,0:T(8,128)(2,1)} %w_ref.1, bf16[128,2048]{1,0:T(8,128)(2,1)} %s_ref.1, f32[1,2048]{1,0:T(1,128)} %bitcast.204, ...), custom_call_target="tpu_custom_call" | custom-call | flops 5000000000 | tf_op jit(solution)/shard_map/project/pallas_call | solution.py:276
  137.8 6.2 %all-to-all-start.3 = ((bf16[32,40,512]{2,1,0:T(8,128)(2,1)}), bf16[32,40,512]{2,1,0:T(8,128)(2,1)S(1)}, u32[]{:S(2)}, u32[]{:S(2)}) async-start(bf16[32,40,512]{2,1,0:T(8,128)(2,1)} %bitcast.189), calls=%async_computation.3 | async-start | bytes 2621440 | tf_op jit(solution)/shard_map/all_to_all | solution.py:540
  144.1 1.4 fusion.5
  145.6 18.5 %all-to-all-done.3 = bf16[32,40,512]{2,1,0:T(8,128)(2,1)S(1)} async-done(((bf16[32,40,512]{2,1,0:T(8,128)(2,1)}), bf16[32,40,512]{2,1,0:T(8,128)(2,1)S(1)}, u32[]{:S(2)}, u32[]{:S(2)}) %all-to-all-start.3) | async-done | bytes 1310752 | tf_op jit(solution)/shard_map/all_to_all | solution.py:540
  164.1 5.4 %all-to-all-start.1 = ((bf16[32,40,512]{2,1,0:T(8,128)(2,1)}), bf16[32,40,512]{2,1,0:T(8,128)(2,1)S(1)}, u32[]{:S(2)}, u32[]{:S(2)}) async-start(bf16[32,40,512]{2,1,0:T(8,128)(2,1)} %bitcast.33), calls=%async_computation.1 | async-start | bytes 2621440 | tf_op jit(solution)/shard_map/all_to_all | solution.py:540
  169.6 18.0 %expert.3 = bf16[2,640,512]{2,1,0:T(8,128)(2,1)} custom-call(bf16[2,640,512]{2,1,0:T(8,128)(2,1)} %bitcast.190, bf16[640,640]{1,0:T(8,128)(2,1)} %get-tuple-element.62.refs_1_, bf16[640,640]{1,0:T(8,128)(2,1)} %get-tuple-element.61.refs_2_, bf16[2048,640]{1,0:T(8,128)(2,1)} %bitcast.refs_3_, bf16[2048,640]{1,0:T(8,128)(2,1)} %bitcast.1.refs_4_, ...), custom_call_target="tpu_custom_call" | custom-call | flops 16000000000 | tf_op jit(solution)/shard_map/expert/pallas_call | solution.py:371
  187.6 1.3 all-to-all-done.1
  188.9 7.8 %all-to-all-start.4 = ((bf16[32,40,512]{2,1,0:T(8,128)(2,1)}), bf16[32,40,512]{2,1,0:T(8,128)(2,1)S(1)}, u32[]{:S(2)}, u32[]{:S(2)}) async-start(bf16[32,40,512]{2,1,0:T(8,128)(2,1)} %bitcast.192), calls=%async_computation.4 | async-start | bytes 2621440 | tf_op jit(solution)/shard_map/all_to_all | solution.py:540
  196.7 18.1 %expert.2 = bf16[2,640,512]{2,1,0:T(8,128)(2,1)} custom-call(bf16[2,640,512]{2,1,0:T(8,128)(2,1)} %bitcast.191, bf16[640,640]{1,0:T(8,128)(2,1)} %get-tuple-element.62.refs_1_, bf16[640,640]{1,0:T(8,128)(2,1)} %get-tuple-element.61.refs_2_, bf16[2048,640]{1,0:T(8,128)(2,1)} %bitcast.refs_3_, bf16[2048,640]{1,0:T(8,128)(2,1)} %bitcast.1.refs_4_, ...), custom_call_target="tpu_custom_call" | custom-call | flops 16000000000 | tf_op jit(solution)/shard_map/expert/pallas_call | solution.py:371
  215.4 8.8 %all-to-all-start.2 = ((bf16[32,40,512]{2,1,0:T(8,128)(2,1)}), bf16[32,40,512]{2,1,0:T(8,128)(2,1)S(1)}, u32[]{:S(2)}, u32[]{:S(2)}) async-start(bf16[32,40,512]{2,1,0:T(8,128)(2,1)} %bitcast.188), calls=%async_computation.2 | async-start | bytes 2621440 | tf_op jit(solution)/shard_map/all_to_all | solution.py:540
  224.3 1.0 fusion.1
  225.3 1.6 pad_maximum_fusion.refs_2_
  227.0 15.4 %all-to-all-done.2 = bf16[32,40,512]{2,1,0:T(8,128)(2,1)S(1)} async-done(((bf16[32,40,512]{2,1,0:T(8,128)(2,1)}), bf16[32,40,512]{2,1,0:T(8,128)(2,1)S(1)}, u32[]{:S(2)}, u32[]{:S(2)}) %all-to-all-start.2) | async-done | bytes 1310752 | tf_op jit(solution)/shard_map/all_to_all | solution.py:540
  242.4 1.1 copy-done.2
  243.4 5.9 %combine.1 = bf16[128,2048]{1,0:T(8,128)(2,1)} custom-call(bf16[2,640,512]{2,1,0:T(8,128)(2,1)} %bitcast.187, bf16[2,640,512]{2,1,0:T(8,128)(2,1)} %bitcast.186, bf16[4,256,1280]{2,1,0:T(8,128)(2,1)} %pad_maximum_fusion.refs_2_, f32[128,2048]{1,0:T(8,128)} %get-tuple-element.38.refs_3_), custom_call_target="tpu_custom_call" | custom-call | tf_op jit(solution)/shard_map/combine/pallas_call | solution.py:412
  (98 shorter events, 8.1 us)
Async XLA Ops:
  0.0 9.4 %copy-start.5 = (bf16[1024,128]{1,0:T(8,128)(2,1)S(1)}, bf16[1024,128]{1,0:T(8,128)(2,1)}, u32[]{:S(2)}) copy-start(bf16[1024,128]{1,0:T(8,128)(2,1)} %param.13) | copy-start | bytes 786436
  0.0 11.9 %copy-start.6 = (s32[128,2]{0,1:T(2,128)S(1)}, s32[128,2]{0,1:T(2,128)}, u32[]{:S(2)}) copy-start(s32[128,2]{0,1:T(2,128)} %param.21) | copy-start | bytes 3076
  2.9 10.5 %collective-permute-start.12 = (bf16[512,256]{1,0:T(8,128)(2,1)S(1)}, bf16[512,256]{1,0:T(8,128)(2,1)S(1)}, u32[]{:S(2)}, u32[]{:S(2)}) collective-permute-start(bf16[512,256]{1,0:T(8,128)(2,1)S(1)} %get-tuple-element.51), channel_id=1, source_target_pairs={{0,32},{8,40},{16,48},{24,56},{32,64},{40,72},{48,80},{56,88},{64,... | collective-permute-start | bytes 786440 | tf_op jit(solution)/shard_map/ppermute | solution.py:199
  4.6 11.0 %collective-permute-start.13 = (bf16[512,256]{1,0:T(8,128)(2,1)S(1)}, bf16[512,256]{1,0:T(8,128)(2,1)S(1)}, u32[]{:S(2)}, u32[]{:S(2)}) collective-permute-start(bf16[512,256]{1,0:T(8,128)(2,1)S(1)} %get-tuple-element.51), channel_id=1, source_target_pairs={{0,96},{8,104},{16,112},{24,120},{32,0},{40,8},{48,16},{56,24},{64... | collective-permute-start | bytes 786440 | tf_op jit(solution)/shard_map/ppermute | solution.py:199
  6.7 9.7 %collective-permute-start.4 = (bf16[512,256]{1,0:T(8,128)(2,1)S(1)}, bf16[512,256]{1,0:T(8,128)(2,1)S(1)}, u32[]{:S(2)}, u32[]{:S(2)}) collective-permute-start(bf16[512,256]{1,0:T(8,128)(2,1)S(1)} %get-tuple-element.54), channel_id=1, source_target_pairs={{0,8},{8,16},{16,24},{24,0},{32,40},{40,48},{48,56},{56,32},{64,72... | collective-permute-start | bytes 786440 | tf_op jit(solution)/shard_map/ppermute | solution.py:199
  7.9 11.9 %collective-permute-start.5 = (bf16[512,256]{1,0:T(8,128)(2,1)S(1)}, bf16[512,256]{1,0:T(8,128)(2,1)S(1)}, u32[]{:S(2)}, u32[]{:S(2)}) collective-permute-start(bf16[512,256]{1,0:T(8,128)(2,1)S(1)} %get-tuple-element.54), channel_id=1, source_target_pairs={{0,24},{8,0},{16,8},{24,16},{32,56},{40,32},{48,40},{56,48},{64,88... | collective-permute-start | bytes 786440 | tf_op jit(solution)/shard_map/ppermute | solution.py:199
  9.4 23.6 %collective-permute-start.3 = (bf16[512,128]{1,0:T(8,128)(2,1)S(1)}, bf16[512,128]{1,0:T(8,128)(2,1)S(1)}, u32[]{:S(2)}, u32[]{:S(2)}) collective-permute-start(bf16[512,128]{1,0:T(8,128)(2,1)S(1)} %bitcast.199), channel_id=1, source_target_pairs={{0,120},{8,112},{16,104},{24,96},{32,88},{40,80},{48,72},{56,64},{... | collective-permute-start | bytes 393224 | tf_op jit(solution)/shard_map/ppermute | solution.py:221
  12.8 18.8 %copy-start.7 = (s32[128,1]{0,1:T(1,128)}, s32[128,1]{0,1:T(1,128)S(1)}, u32[]{:S(2)}) copy-start(s32[128,1]{0,1:T(1,128)S(1)} %copy.62) | copy-start | bytes 1540
  13.4 123.4 %collective-permute-start = (bf16[2048,640]{1,0:T(8,128)(2,1)}, bf16[2048,640]{1,0:T(8,128)(2,1)}, u32[]{:S(2)}, u32[]{:S(2)}) collective-permute-start(bf16[2048,640]{1,0:T(8,128)(2,1)} %bitcast.refs_3_), channel_id=1, source_target_pairs={{0,6},{1,3},{2,0},{3,5},{4,2},{5,7},{6,4},{7,1},{8,14},{9,11},{10,... | collective-permute-start | bytes 7864328 | tf_op jit(solution)/shard_map/ppermute | solution.py:459
  15.5 6.5 %collective-permute-start.14 = (bf16[256,256]{1,0:T(8,128)(2,1)S(1)}, bf16[256,256]{1,0:T(8,128)(2,1)S(1)}, u32[]{:S(2)}, u32[]{:S(2)}) collective-permute-start(bf16[256,256]{1,0:T(8,128)(2,1)S(1)} %slice.92), channel_id=1, source_target_pairs={{0,32},{8,40},{16,48},{24,56},{32,64},{40,72},{48,80},{56,88},{64,... | collective-permute-start | bytes 393224 | tf_op jit(solution)/shard_map/ppermute | solution.py:200
  16.4 9.3 %collective-permute-start.15 = (bf16[256,256]{1,0:T(8,128)(2,1)S(1)}, bf16[256,256]{1,0:T(8,128)(2,1)S(1)}, u32[]{:S(2)}, u32[]{:S(2)}) collective-permute-start(bf16[256,256]{1,0:T(8,128)(2,1)S(1)} %slice.93), channel_id=1, source_target_pairs={{0,96},{8,104},{16,112},{24,120},{32,0},{40,8},{48,16},{56,24},{64... | collective-permute-start | bytes 393224 | tf_op jit(solution)/shard_map/ppermute | solution.py:200
  19.8 6.6 %collective-permute-start.6 = (bf16[256,256]{1,0:T(8,128)(2,1)S(1)}, bf16[256,256]{1,0:T(8,128)(2,1)S(1)}, u32[]{:S(2)}, u32[]{:S(2)}) collective-permute-start(bf16[256,256]{1,0:T(8,128)(2,1)S(1)} %slice.87), channel_id=1, source_target_pairs={{0,8},{8,16},{16,24},{24,0},{32,40},{40,48},{48,56},{56,32},{64,72... | collective-permute-start | bytes 393224 | tf_op jit(solution)/shard_map/ppermute | solution.py:200
  22.0 7.7 %collective-permute-start.7 = (bf16[256,256]{1,0:T(8,128)(2,1)S(1)}, bf16[256,256]{1,0:T(8,128)(2,1)S(1)}, u32[]{:S(2)}, u32[]{:S(2)}) collective-permute-start(bf16[256,256]{1,0:T(8,128)(2,1)S(1)} %slice.88), channel_id=1, source_target_pairs={{0,24},{8,0},{16,8},{24,16},{32,56},{40,32},{48,40},{56,48},{64,88... | collective-permute-start | bytes 393224 | tf_op jit(solution)/shard_map/ppermute | solution.py:200
  26.4 25.1 %collective-permute-start.16 = (bf16[2048,256]{1,0:T(8,128)(2,1)}, bf16[2048,256]{1,0:T(8,128)(2,1)S(1)}, u32[]{:S(2)}, u32[]{:S(2)}) collective-permute-start(bf16[2048,256]{1,0:T(8,128)(2,1)} %constant_dynamic-update-slice_fusion.7.refs_5_), channel_id=1, source_target_pairs={{0,8},{8,16},{16,24},{24,0},{32,40},{40,48},{48,56},{56,32},{64,72... | collective-permute-start | bytes 3145736 | tf_op jit(solution)/shard_map/ppermute | solution.py:199
  26.4 25.2 %collective-permute-start.18 = (bf16[2048,256]{1,0:T(8,128)(2,1)}, bf16[2048,256]{1,0:T(8,128)(2,1)S(1)}, u32[]{:S(2)}, u32[]{:S(2)}) collective-permute-start(bf16[2048,256]{1,0:T(8,128)(2,1)} %constant_dynamic-update-slice_fusion.7.refs_5_), channel_id=1, source_target_pairs={{0,24},{8,0},{16,8},{24,16},{32,56},{40,32},{48,40},{56,48},{64,88... | collective-permute-start | bytes 3145736 | tf_op jit(solution)/shard_map/ppermute | solution.py:199
  30.4 24.0 %collective-permute-start.10 = (bf16[2048,256]{1,0:T(8,128)(2,1)}, bf16[2048,256]{1,0:T(8,128)(2,1)S(1)}, u32[]{:S(2)}, u32[]{:S(2)}) collective-permute-start(bf16[2048,256]{1,0:T(8,128)(2,1)} %constant_dynamic-update-slice_fusion.2.refs_4_), channel_id=1, source_target_pairs={{0,96},{8,104},{16,112},{24,120},{32,0},{40,8},{48,16},{56,24},{64... | collective-permute-start | bytes 3145736 | tf_op jit(solution)/shard_map/ppermute | solution.py:199
  33.0 32.2 %collective-permute-start.8 = (bf16[2048,256]{1,0:T(8,128)(2,1)}, bf16[2048,256]{1,0:T(8,128)(2,1)S(1)}, u32[]{:S(2)}, u32[]{:S(2)}) collective-permute-start(bf16[2048,256]{1,0:T(8,128)(2,1)} %constant_dynamic-update-slice_fusion.2.refs_4_), channel_id=1, source_target_pairs={{0,32},{8,40},{16,48},{24,56},{32,64},{40,72},{48,80},{56,88},{64,... | collective-permute-start | bytes 3145736 | tf_op jit(solution)/shard_map/ppermute | solution.py:199
  34.5 20.6 %copy-start = (f32[128]{0:T(128)S(1)}, f32[128]{0:T(128)}, u32[]{:S(2)}) copy-start(f32[128]{0:T(128)} %param.17) | copy-start | bytes 1540
  51.5 14.0 %collective-permute-start.17 = (bf16[1024,256]{1,0:T(8,128)(2,1)S(1)}, bf16[1024,256]{1,0:T(8,128)(2,1)S(1)}, u32[]{:S(2)}, u32[]{:S(2)}) collective-permute-start(bf16[1024,256]{1,0:T(8,128)(2,1)S(1)} %slice.94), channel_id=1, source_target_pairs={{0,8},{8,16},{16,24},{24,0},{32,40},{40,48},{48,56},{56,32},{64,72... | collective-permute-start | bytes 1572872 | tf_op jit(solution)/shard_map/ppermute | solution.py:200
  51.6 13.9 %collective-permute-start.19 = (bf16[1024,256]{1,0:T(8,128)(2,1)S(1)}, bf16[1024,256]{1,0:T(8,128)(2,1)S(1)}, u32[]{:S(2)}, u32[]{:S(2)}) collective-permute-start(bf16[1024,256]{1,0:T(8,128)(2,1)S(1)} %slice.95), channel_id=1, source_target_pairs={{0,24},{8,0},{16,8},{24,16},{32,56},{40,32},{48,40},{56,48},{64,88... | collective-permute-start | bytes 1572872 | tf_op jit(solution)/shard_map/ppermute | solution.py:200
  54.4 15.7 %collective-permute-start.11 = (bf16[1024,256]{1,0:T(8,128)(2,1)S(1)}, bf16[1024,256]{1,0:T(8,128)(2,1)S(1)}, u32[]{:S(2)}, u32[]{:S(2)}) collective-permute-start(bf16[1024,256]{1,0:T(8,128)(2,1)S(1)} %slice.90), channel_id=1, source_target_pairs={{0,96},{8,104},{16,112},{24,120},{32,0},{40,8},{48,16},{56,24},{64... | collective-permute-start | bytes 1572872 | tf_op jit(solution)/shard_map/ppermute | solution.py:200
  65.2 71.9 %collective-permute-start.1 = (bf16[2048,640]{1,0:T(8,128)(2,1)}, bf16[2048,640]{1,0:T(8,128)(2,1)}, u32[]{:S(2)}, u32[]{:S(2)}) collective-permute-start(bf16[2048,640]{1,0:T(8,128)(2,1)} %bitcast.1.refs_4_), channel_id=1, source_target_pairs={{0,6},{1,3},{2,0},{3,5},{4,2},{5,7},{6,4},{7,1},{8,14},{9,11},{10,... | collective-permute-start | bytes 7864328 | tf_op jit(solution)/shard_map/ppermute | solution.py:459
  65.5 71.7 %collective-permute-start.2 = (bf16[640,2048]{1,0:T(8,128)(2,1)}, bf16[640,2048]{1,0:T(8,128)(2,1)}, u32[]{:S(2)}, u32[]{:S(2)}) collective-permute-start(bf16[640,2048]{1,0:T(8,128)(2,1)} %bitcast.2.refs_5_), channel_id=1, source_target_pairs={{0,6},{1,3},{2,0},{3,5},{4,2},{5,7},{6,4},{7,1},{8,14},{9,11},{10,... | collective-permute-start | bytes 7864328 | tf_op jit(solution)/shard_map/ppermute | solution.py:459
  65.6 72.1 %collective-permute-start.20 = (bf16[2048,640]{1,0:T(8,128)(2,1)}, bf16[2048,640]{1,0:T(8,128)(2,1)}, u32[]{:S(2)}, u32[]{:S(2)}) collective-permute-start(bf16[2048,640]{1,0:T(8,128)(2,1)} %bitcast.refs_3_), channel_id=1, source_target_pairs={{0,1},{1,0},{2,3},{3,2},{4,5},{5,4},{6,7},{7,6},{8,9},{9,8},{10,11... | collective-permute-start | bytes 7864328 | tf_op jit(solution)/shard_map/ppermute | solution.py:508
  70.1 15.9 %collective-permute-start.9 = (bf16[1024,256]{1,0:T(8,128)(2,1)S(1)}, bf16[1024,256]{1,0:T(8,128)(2,1)S(1)}, u32[]{:S(2)}, u32[]{:S(2)}) collective-permute-start(bf16[1024,256]{1,0:T(8,128)(2,1)S(1)} %slice.89), channel_id=1, source_target_pairs={{0,32},{8,40},{16,48},{24,56},{32,64},{40,72},{48,80},{56,88},{64,... | collective-permute-start | bytes 1572872 | tf_op jit(solution)/shard_map/ppermute | solution.py:200
  94.0 36.3 %all-to-all-start = ((bf16[16,64,128]{2,1,0:T(8,128)(2,1)}), bf16[16,64,128]{2,1,0:T(8,128)(2,1)S(1)}, u32[]{:S(2)}, u32[]{:S(2)}) async-start(bf16[16,64,128]{2,1,0:T(8,128)(2,1)} %bitcast.12), calls=%async_computation | async-start | bytes 524288 | tf_op jit(solution)/shard_map/all_to_all | solution.py:516
  105.2 64.3 %collective-permute-start.21 = (bf16[2048,640]{1,0:T(8,128)(2,1)}, bf16[2048,640]{1,0:T(8,128)(2,1)}, u32[]{:S(2)}, u32[]{:S(2)}) collective-permute-start(bf16[2048,640]{1,0:T(8,128)(2,1)} %bitcast.1.refs_4_), channel_id=1, source_target_pairs={{0,1},{1,0},{2,3},{3,2},{4,5},{5,4},{6,7},{7,6},{8,9},{9,8},{10,11... | collective-permute-start | bytes 7864328 | tf_op jit(solution)/shard_map/ppermute | solution.py:508
  136.8 32.7 %collective-permute-start.22 = (bf16[640,2048]{1,0:T(8,128)(2,1)}, bf16[640,2048]{1,0:T(8,128)(2,1)}, u32[]{:S(2)}, u32[]{:S(2)}) collective-permute-start(bf16[640,2048]{1,0:T(8,128)(2,1)} %bitcast.2.refs_5_), channel_id=1, source_target_pairs={{0,1},{1,0},{2,3},{3,2},{4,5},{5,4},{6,7},{7,6},{8,9},{9,8},{10,11... | collective-permute-start | bytes 7864328 | tf_op jit(solution)/shard_map/ppermute | solution.py:508
  137.1 32.4 %collective-permute-start.23 = (bf16[2048,640]{1,0:T(8,128)(2,1)}, bf16[2048,640]{1,0:T(8,128)(2,1)}, u32[]{:S(2)}, u32[]{:S(2)}) collective-permute-start(bf16[2048,640]{1,0:T(8,128)(2,1)} %collective-permute-done.refs_9_), channel_id=1, source_target_pairs={{0,1},{1,0},{2,3},{3,2},{4,5},{5,4},{6,7},{7,6},{8,9},{9,8},{10,11... | collective-permute-start | bytes 7864328 | tf_op jit(solution)/shard_map/ppermute | solution.py:524
  137.3 32.2 %collective-permute-start.24 = (bf16[2048,640]{1,0:T(8,128)(2,1)}, bf16[2048,640]{1,0:T(8,128)(2,1)}, u32[]{:S(2)}, u32[]{:S(2)}) collective-permute-start(bf16[2048,640]{1,0:T(8,128)(2,1)} %collective-permute-done.1.refs_10_), channel_id=1, source_target_pairs={{0,1},{1,0},{2,3},{3,2},{4,5},{5,4},{6,7},{7,6},{8,9},{9,8},{10,11... | collective-permute-start | bytes 7864328 | tf_op jit(solution)/shard_map/ppermute | solution.py:524
  137.7 31.9 %collective-permute-start.25 = (bf16[640,2048]{1,0:T(8,128)(2,1)}, bf16[640,2048]{1,0:T(8,128)(2,1)}, u32[]{:S(2)}, u32[]{:S(2)}) collective-permute-start(bf16[640,2048]{1,0:T(8,128)(2,1)} %collective-permute-done.2.refs_11_), channel_id=1, source_target_pairs={{0,1},{1,0},{2,3},{3,2},{4,5},{5,4},{6,7},{7,6},{8,9},{9,8},{10,11... | collective-permute-start | bytes 7864328 | tf_op jit(solution)/shard_map/ppermute | solution.py:524
  137.8 26.3 %all-to-all-start.3 = ((bf16[32,40,512]{2,1,0:T(8,128)(2,1)}), bf16[32,40,512]{2,1,0:T(8,128)(2,1)S(1)}, u32[]{:S(2)}, u32[]{:S(2)}) async-start(bf16[32,40,512]{2,1,0:T(8,128)(2,1)} %bitcast.189), calls=%async_computation.3 | async-start | bytes 2621440 | tf_op jit(solution)/shard_map/all_to_all | solution.py:540
  164.1 5.4 %copy-start.3 = (bf16[32,40,512]{2,1,0:T(8,128)(2,1)}, bf16[32,40,512]{2,1,0:T(8,128)(2,1)S(1)}, u32[]{:S(2)}) copy-start(bf16[32,40,512]{2,1,0:T(8,128)(2,1)S(1)} %all-to-all-done.3) | copy-start | bytes 3932164
  164.1 24.7 %all-to-all-start.1 = ((bf16[32,40,512]{2,1,0:T(8,128)(2,1)}), bf16[32,40,512]{2,1,0:T(8,128)(2,1)S(1)}, u32[]{:S(2)}, u32[]{:S(2)}) async-start(bf16[32,40,512]{2,1,0:T(8,128)(2,1)} %bitcast.33), calls=%async_computation.1 | async-start | bytes 2621440 | tf_op jit(solution)/shard_map/all_to_all | solution.py:540
  188.8 7.8 %copy-start.4 = (bf16[32,40,512]{2,1,0:T(8,128)(2,1)}, bf16[32,40,512]{2,1,0:T(8,128)(2,1)S(1)}, u32[]{:S(2)}) copy-start(bf16[32,40,512]{2,1,0:T(8,128)(2,1)S(1)} %all-to-all-done.1) | copy-start | bytes 3932164
  188.9 26.6 %all-to-all-start.4 = ((bf16[32,40,512]{2,1,0:T(8,128)(2,1)}), bf16[32,40,512]{2,1,0:T(8,128)(2,1)S(1)}, u32[]{:S(2)}, u32[]{:S(2)}) async-start(bf16[32,40,512]{2,1,0:T(8,128)(2,1)} %bitcast.192), calls=%async_computation.4 | async-start | bytes 2621440 | tf_op jit(solution)/shard_map/all_to_all | solution.py:540
  214.8 9.4 %copy-start.8 = (s32[128,1]{0,1:T(1,128)S(1)}, s32[128,1]{0,1:T(1,128)}, u32[]{:S(2)}) copy-start(s32[128,1]{0,1:T(1,128)} %copy-done.7) | copy-start | bytes 1540
  214.8 9.4 %copy-start.11 = (s32[1,128]{1,0:T(1,128)S(1)}, s32[1,128]{1,0:T(1,128)}, u32[]{:S(2)}) copy-start(s32[1,128]{1,0:T(1,128)} %get-tuple-element.40) | copy-start | bytes 1540
  214.8 9.4 %copy-start.12 = (s32[1,128]{1,0:T(1,128)S(1)}, s32[1,128]{1,0:T(1,128)}, u32[]{:S(2)}) copy-start(s32[1,128]{1,0:T(1,128)} %get-tuple-element.99) | copy-start | bytes 1540
  214.9 9.4 %copy-start.9 = (s32[1,128]{1,0:T(1,128)S(1)}, s32[1,128]{1,0:T(1,128)}, u32[]{:S(2)}) copy-start(s32[1,128]{1,0:T(1,128)} %get-tuple-element.39) | copy-start | bytes 1540
  214.9 9.4 %copy-start.10 = (s32[1,128]{1,0:T(1,128)S(1)}, s32[1,128]{1,0:T(1,128)}, u32[]{:S(2)}) copy-start(s32[1,128]{1,0:T(1,128)} %get-tuple-element.98) | copy-start | bytes 1540
  214.9 9.4 %copy-start.13 = (f32[128,2]{0,1:T(2,128)S(1)}, f32[128,2]{0,1:T(2,128)}, u32[]{:S(2)}) copy-start(f32[128,2]{0,1:T(2,128)} %param.22) | copy-start | bytes 3076
  215.4 9.9 %copy-start.1 = (bf16[32,40,512]{2,1,0:T(8,128)(2,1)}, bf16[32,40,512]{2,1,0:T(8,128)(2,1)S(1)}, u32[]{:S(2)}) copy-start(bf16[32,40,512]{2,1,0:T(8,128)(2,1)S(1)} %all-to-all-done.4) | copy-start | bytes 3932164
  215.4 26.9 %all-to-all-start.2 = ((bf16[32,40,512]{2,1,0:T(8,128)(2,1)}), bf16[32,40,512]{2,1,0:T(8,128)(2,1)S(1)}, u32[]{:S(2)}, u32[]{:S(2)}) async-start(bf16[32,40,512]{2,1,0:T(8,128)(2,1)} %bitcast.188), calls=%async_computation.2 | async-start | bytes 2621440 | tf_op jit(solution)/shard_map/all_to_all | solution.py:540
  242.4 1.1 copy-start.2
where the time goes:
time: 253 us; the launch traced here: 249 us
  Pallas kernels  80 us (32%)
  waiting for transfers between devices  77.7 us (31%)
  starting transfers between devices  69.7 us (28%)
  local copies, waits for them, and re-layouts  10.4 us (4%)
  other arithmetic  10.2 us (4%)
    pallas_call x2, Pallas kernels, expert(): pl.pallas_call(lambda *refs: expert_body(len(sets), *refs), in_specs=[pl....  36.2 us
    all_to_all x4, waiting for transfers between devices, exchange(): lax.all_to_all(x, BOTH, split_axis=0, concat_axis=0, tiled=True, axis_ind...  35.7 us
    pallas_call x3, Pallas kernels, attention(): pl.pallas_call(lambda *refs: attention_body(pieces, side, first, final, l...  32.2 us
    all_to_all x4, starting transfers between devices, exchange(): lax.all_to_all(x, BOTH, split_axis=0, concat_axis=0, tiled=True, axis_ind...  28.1 us
    all_to_all x1, waiting for transfers between devices, local(): lax.all_to_all(heads, BOTH, split_axis=0, concat_axis=0, tiled=True, axis...  24.7 us
    ppermute x4, waiting for transfers between devices, spread(): lax.ppermute(array, 'sp', forth)  16.1 us
    all_to_all x1, starting transfers between devices, local(): lax.all_to_all(heads, BOTH, split_axis=0, concat_axis=0, tiled=True, axis...  9.31 us
    ppermute x4, starting transfers between devices, spread(): lax.ppermute(behind[half:], 'sp', back)  9.07 us
  transfers between devices with their start and end apart: 31, of which 7 were waited for; matrix products, arithmetic and copies ran while one was open for 7% of the time, Pallas kernels for 30%

commit v1 on v0

--- a/solution.py
+++ b/solution.py
@@ -122,11 +122,11 @@
             run([(m, r) for r in range(rows // ROWS) for m in range(2)])
         else:
 
-            def some(r, carry):
-                run([(m, r) for m in range(2)])
+            def some(t, carry):
+                run([(t % 2, t // 2)])
                 return carry
 
-            lax.fori_loop(0, rows // ROWS, some, 0)
+            lax.fori_loop(0, 2 * rows // ROWS, some, 0)
 
     def half(h, carry):
         number = bounds[h]
@@ -286,18 +286,26 @@
     return pl.CostEstimate(flops=int(microseconds * FLOPS_US), bytes_accessed=0, transcendentals=0)
 
 
-def expert_body(sets, r_any, s_any, p_any, *refs):
-    weights = refs[: 3 * sets]
-    o_ref, r_ref, s_ref, p_ref, x_sc, act_sc, acc_sc, in_buf, down_buf, sem, small = refs[3 * sets :]
+def expert_body(sizes, r_any, s_any, p_any, *refs):
+    sets = len(sizes)
+    flat, weights = refs, []
+    for size in sizes:
+        weights.append((flat[0], flat[1], flat[2:size]))
+        flat = flat[size:]
+    o_ref, r_ref, s_ref, p_ref, x_sc, act_sc, acc_sc, in_buf, down_buf, sem, small = flat
     hidden = in_buf.shape[2] // 2
     rows = s_ref.shape[0] // CUTS
 
-    def copy(n, kind):
+    def start(n, kind):
         if kind < 2:
             to = in_buf.at[n, :, pl.ds(kind * hidden, hidden)]
+            pltpu.make_async_copy(weights[n][kind], to, sem.at[3 * n + kind]).start()
         else:
-            to = down_buf.at[n // 2, pl.ds(n % 2 * hidden, hidden), :]
-        return pltpu.make_async_copy(weights[3 * n + kind], to, sem.at[3 * n + kind])
+            begin = n % 2 * hidden
+            for piece in weights[n][2]:
+                to = down_buf.at[n // 2, pl.ds(begin, piece.shape[0]), :]
+                pltpu.make_async_copy(piece, to, sem.at[3 * n + 2]).start()
+                begin += piece.shape[0]
 
     def share(h):
         return pl.ds(pl.multiple_of(h * rows, 16), rows)
@@ -307,7 +315,7 @@
             to = in_buf.at[n, :, pl.ds(kind * hidden, hidden)]
         else:
             to = down_buf.at[n // 2, pl.ds(pl.multiple_of(n % 2 * hidden, 128), hidden), :]
-        pltpu.make_async_copy(weights[kind], to, sem.at[3 * n + kind]).wait()
+        pltpu.make_async_copy((weights[0][0], weights[0][1], weights[0][2][0])[kind], to, sem.at[3 * n + kind]).wait()
 
     first = pltpu.make_async_copy(r_any, r_ref, small.at[0])
     second = pltpu.make_async_copy(s_any, s_ref, small.at[1])
@@ -320,11 +328,11 @@
     first.start()
     second.start()
     for n, kind in order[:2]:
-        copy(n, kind).start()
+        start(n, kind)
     first.wait()
     second.wait()
     for n, kind in order[2:]:
-        copy(n, kind).start()
+        start(n, kind)
     third.start()
     wide = r_ref.shape[2]
 
@@ -369,7 +377,7 @@
     width, hidden = sets[0][0].shape
     flat = [w for one in sets for w in one]
     return pl.pallas_call(
-        lambda *refs: expert_body(len(sets), *refs),
+        lambda *refs: expert_body([len(one) for one in sets], *refs),
         in_specs=[pl.BlockSpec(memory_space=pl.ANY)] * (3 + len(flat)),
         out_specs=pl.BlockSpec(memory_space=pltpu.VMEM),
         out_shape=jax.ShapeDtypeStruct(arrived.shape, BF16),
@@ -382,7 +390,7 @@
             pltpu.VMEM((rows, width), F32),
             pltpu.VMEM((len(sets), width, 2 * hidden), BF16),
             pltpu.VMEM((len(sets) // 2, 2 * hidden, width), BF16),
-            pltpu.SemaphoreType.DMA((len(flat),)),
+            pltpu.SemaphoreType.DMA((3 * len(sets),)),
             pltpu.SemaphoreType.DMA((3,)),
         ],
         compiler_params=pltpu.CompilerParams(vmem_limit_bytes=VMEM_LIMIT),
@@ -455,7 +463,9 @@
     along = moved(sp_size, tp_size, lambda c: 2 * c - 1, 0)
     sibling = moved(sp_size, tp_size, lambda c: 0, 1)
     passed = []
-    for w in mine:
+    gate, up, down = mine
+    later = down.shape[0] // 2
+    for w in (gate, up, down[:later]):
         passed.append(lax.ppermute(w, BOTH, along))
     passed = tuple(passed)
 
@@ -518,11 +528,14 @@
     ).reshape(2, tp_size, half, 128)
     heads = jnp.where(low, heads, heads[::-1])
 
+    rest, heads = lax.optimization_barrier((down[later:], heads))
+    rest = lax.ppermute(rest, BOTH, along)
     attended, *outgoing = project(heads, out_weight, stream, ffn_gain, dispatch)
 
     passed, outgoing = lax.optimization_barrier((passed, outgoing))
     passed_too = tuple(lax.ppermute(w, BOTH, sibling) for w in passed)
-    sets = (mine, mine_too, passed, passed_too)
+    rest_too = lax.ppermute(rest, BOTH, sibling)
+    sets = (mine, mine_too, passed + (rest,), passed_too + (rest_too,))
 
     ring = tp_size // 2
     members = [
@@ -541,7 +554,9 @@
             x, BOTH, split_axis=0, concat_axis=0, tiled=True, axis_index_groups=members
         ).reshape(SHARERS, packed, width // CUTS)
 
-    arrived = [exchange(x) for x in outgoing]
+    arrived = []
+    for x in outgoing:
+        arrived.append(exchange(x))
     returned = [exchange(expert(x, select, place, sets)) for x in arrived]
     return combine(returned, weights, attended)
 

time: 253 us -> 274 us (1.083)
  waiting for transfers between devices: 77.7 us -> 94.9 us
  starting transfers between devices: 69.7 us -> 74.7 us
  other arithmetic: 10.2 us -> 7.07 us
    ppermute x4, waiting for transfers between devices: 1.06 us -> 22.1 us  [spread(): lax.ppermute(before[:half], 'sp', forth)]
    ppermute x0 -> x2, waiting for transfers between devices: none -> 15.7 us  [the longest x1 15.7 us: local(): rest = lax.ppermute(rest, BOTH, along)]
    ppermute x4, waiting for transfers between devices: 16.1 us -> 2.26 us  [spread(): lax.ppermute(array, 'sp', forth)]
    all_to_all x1, waiting for transfers between devices: 24.7 us -> 13 us  [local(): lax.all_to_all(heads, BOTH, split_axis=0, concat_axis=0, tiled=True, axis...]
    ppermute x4, waiting for transfers between devices: 0.01 us -> 5.92 us  [spread(): lax.ppermute(array, 'sp', back)]
    slice x0 -> x1, local copies, waits for them, and re-layouts: none -> 3.6 us  [local(): rest, heads = lax.optimization_barrier((down[later:], heads))]
    unnamed x38 -> x28, local copies, waits for them, and re-layouts: 6.65 us -> 3.35 us
  transfers between devices with their start and end apart: 31 -> 33, of which waited for: 7 -> 10; matrix products, arithmetic and copies ran while one was open for 7% -> 5% of each run, Pallas kernels for 30% -> 28%
where the time goes in v1:
time: 274 us; the launch traced here: 270 us
  waiting for transfers between devices  94.9 us (35%)
  Pallas kernels  81.3 us (30%)
  starting transfers between devices  74.7 us (27%)
  local copies, waits for them, and re-layouts  10.6 us (4%)
  other arithmetic  7.07 us (3%)
    pallas_call x2, Pallas kernels, expert(): pl.pallas_call(lambda *refs: expert_body([len(one) for one in sets], *ref...  36.8 us
    all_to_all x4, waiting for transfers between devices, exchange(): lax.all_to_all(x, BOTH, split_axis=0, concat_axis=0, tiled=True, axis_ind...  35.9 us
    pallas_call x3, Pallas kernels, attention(): pl.pallas_call(lambda *refs: attention_body(pieces, side, first, final, l...  32.7 us
    all_to_all x4, starting transfers between devices, exchange(): lax.all_to_all(x, BOTH, split_axis=0, concat_axis=0, tiled=True, axis_ind...  30.2 us
    ppermute x4, waiting for transfers between devices, spread(): lax.ppermute(before[:half], 'sp', forth)  22.1 us
    ppermute x1, waiting for transfers between devices, local(): rest = lax.ppermute(rest, BOTH, along)  15.7 us
    all_to_all x1, waiting for transfers between devices, local(): lax.all_to_all(heads, BOTH, split_axis=0, concat_axis=0, tiled=True, axis...  13 us
    all_to_all x1, starting transfers between devices, local(): lax.all_to_all(heads, BOTH, split_axis=0, concat_axis=0, tiled=True, axis...  10.1 us
  transfers between devices with their start and end apart: 33, of which 10 were waited for; matrix products, arithmetic and copies ran while one was open for 5% of the time, Pallas kernels for 28%

profile of v1, /device:TPU:9, one launch (start us, length us, event | category | flops | bytes accessed | tf_op | source)
XLA Modules:
  0.0 270.0 jit_solution(1947531899615213094)
XLA Ops:
  0.0 1.0 constant_dynamic-update-slice_fusion.1
  1.0 1.0 constant_dynamic-update-slice_fusion
  2.1 0.9 fusion.32
  2.9 1.6 collective-permute-start.12
  4.6 2.1 collective-permute-start.13
  6.7 1.2 collective-permute-start.4
  7.9 1.5 collective-permute-start.5
  10.0 2.4 collective-permute-start.3
  13.7 0.9 copy.61
  14.7 3.6 %slice_bitcast_fusion = (bf16[320,2048]{1,0:T(8,128)(2,1)}, bf16[320,2048]{1,0:T(8,128)(2,1)}) fusion(bf16[1,640,2048]{2,1,0:T(8,128)(2,1)} %param.25), kind=kLoop, calls=%fused_computation.16 | loop fusion | bytes 5242880 | tf_op jit(solution)/shard_map/slice | solution.py:531
  19.2 2.7 %collective-permute-start.15 = (bf16[256,256]{1,0:T(8,128)(2,1)S(1)}, bf16[256,256]{1,0:T(8,128)(2,1)S(1)}, u32[]{:S(2)}, u32[]{:S(2)}) collective-permute-start(bf16[256,256]{1,0:T(8,128)(2,1)S(1)} %slice.109), channel_id=1, source_target_pairs={{0,96},{8,104},{16,112},{24,120},{32,0},{40,8},{48,16},{56,24},{64... | collective-permute-start | bytes 393224 | tf_op jit(solution)/shard_map/ppermute | solution.py:200
  22.0 2.2 collective-permute-done.14
  24.3 2.7 collective-permute-start.18
  27.2 2.7 %collective-permute-start.7 = (bf16[256,256]{1,0:T(8,128)(2,1)S(1)}, bf16[256,256]{1,0:T(8,128)(2,1)S(1)}, u32[]{:S(2)}, u32[]{:S(2)}) collective-permute-start(bf16[256,256]{1,0:T(8,128)(2,1)S(1)} %slice.104), channel_id=1, source_target_pairs={{0,24},{8,0},{16,8},{24,16},{32,56},{40,32},{48,40},{56,48},{64,88... | collective-permute-start | bytes 393224 | tf_op jit(solution)/shard_map/ppermute | solution.py:200
  29.9 19.9 %collective-permute-done.6 = bf16[256,256]{1,0:T(8,128)(2,1)S(1)} collective-permute-done((bf16[256,256]{1,0:T(8,128)(2,1)S(1)}, bf16[256,256]{1,0:T(8,128)(2,1)S(1)}, u32[]{:S(2)}, u32[]{:S(2)}) %collective-permute-start.6) | collective-permute-done | bytes 131104 | tf_op jit(solution)/shard_map/ppermute | solution.py:200
  49.8 1.3 collective-permute-start
  51.2 2.5 collective-permute-start.10
  54.1 2.7 %collective-permute-start.19 = (bf16[1024,256]{1,0:T(8,128)(2,1)S(1)}, bf16[1024,256]{1,0:T(8,128)(2,1)S(1)}, u32[]{:S(2)}, u32[]{:S(2)}) collective-permute-start(bf16[1024,256]{1,0:T(8,128)(2,1)S(1)} %slice.111), channel_id=1, source_target_pairs={{0,24},{8,0},{16,8},{24,16},{32,56},{40,32},{48,40},{56,48},{64,88... | collective-permute-start | bytes 1572872 | tf_op jit(solution)/shard_map/ppermute | solution.py:200
  56.8 10.1 %attention.3 = (f32[2,2,512,128]{3,2,1,0:T(8,128)S(1)}, f32[2,2,512,256]{3,2,1,0:T(8,128)S(1)}) custom-call(s32[1]{0:T(128)} %bitcast.4.refs_0_, f32[1]{0:T(128)S(6)} %copy.72.refs_1_, f32[1,128]{1,0:T(1,128)S(1)} %bitcast.187, bf16[2,2,512,128]{3,2,1,0:T(8,128)(2,1)S(1)} %pad_maximum_fusion.1.refs_3_, ...), custom_call_target="tpu_custom_call" | custom-call | flops 8000000000 | tf_op jit(solution)/shard_map/attention/pallas_call | solution.py:183
  66.9 5.9 %collective-permute-done.10.refs_5_ = bf16[2048,256]{1,0:T(8,128)(2,1)S(1)} collective-permute-done((bf16[2048,256]{1,0:T(8,128)(2,1)S(1)}, bf16[2048,256]{1,0:T(8,128)(2,1)S(1)}, u32[]{:S(2)}, u32[]{:S(2)}) %collective-permute-start.10) | collective-permute-done | bytes 1048608 | tf_op jit(solution)/shard_map/ppermute | solution.py:199
  72.8 0.7 collective-permute-start.1
  73.6 2.3 collective-permute-done.8.refs_4_
  75.8 4.7 %collective-permute-start.20 = (bf16[2048,640]{1,0:T(8,128)(2,1)}, bf16[2048,640]{1,0:T(8,128)(2,1)}, u32[]{:S(2)}, u32[]{:S(2)}) collective-permute-start(bf16[2048,640]{1,0:T(8,128)(2,1)} %bitcast.refs_3_), channel_id=1, source_target_pairs={{0,1},{1,0},{2,3},{3,2},{4,5},{5,4},{6,7},{7,6},{8,9},{9,8},{10,11... | collective-permute-start | bytes 7864328 | tf_op jit(solution)/shard_map/ppermute | solution.py:518
  81.2 0.9 collective-permute-start.9
  82.1 15.1 %attention.4 = (f32[2,2,512,128]{3,2,1,0:T(8,128)S(1)}, f32[2,2,512,256]{3,2,1,0:T(8,128)S(1)}) custom-call(s32[1]{0:T(128)} %bitcast.4.refs_0_, f32[1]{0:T(128)S(6)} %copy.72.refs_1_, f32[1,128]{1,0:T(1,128)S(1)} %bitcast.188, bf16[2,2,512,128]{3,2,1,0:T(8,128)(2,1)S(1)} %pad_maximum_fusion.1.refs_3_, bf16[2048,256]{1,0:T(8,128)(2,1)S(1)} %collective-permute-done.8.refs_4_, ...), custom_call_target="tpu_custom_call" | custom-call | flops 16000000000 | tf_op jit(solution)/shard_map/attention/pallas_call | solution.py:183
  97.2 1.1 collective-permute-start.2
  98.4 7.4 %attention.5 = bf16[2,512,128]{2,1,0:T(8,128)(2,1)} custom-call(s32[1]{0:T(128)} %bitcast.4.refs_0_, f32[1]{0:T(128)S(6)} %copy.72.refs_1_, f32[1,128]{1,0:T(1,128)S(1)} %bitcast.189, bf16[2,2,512,128]{3,2,1,0:T(8,128)(2,1)S(1)} %pad_maximum_fusion.1.refs_3_, bf16[1024,256]{1,0:T(8,128)(2,1)S(1)} %collective-permute-done.9.refs_4_, ...), custom_call_target="tpu_custom_call" | custom-call | flops 8000000000 | tf_op jit(solution)/shard_map/attention/pallas_call | solution.py:183
  105.9 10.1 %all-to-all-start = ((bf16[16,64,128]{2,1,0:T(8,128)(2,1)}), bf16[16,64,128]{2,1,0:T(8,128)(2,1)S(1)}, u32[]{:S(2)}, u32[]{:S(2)}) async-start(bf16[16,64,128]{2,1,0:T(8,128)(2,1)} %bitcast.14), calls=%async_computation | async-start | bytes 524288 | tf_op jit(solution)/shard_map/all_to_all | solution.py:526
  116.0 1.9 fusion.6.d_ref
  117.9 13.0 %all-to-all-done = bf16[16,64,128]{2,1,0:T(8,128)(2,1)S(1)} async-done(((bf16[16,64,128]{2,1,0:T(8,128)(2,1)}), bf16[16,64,128]{2,1,0:T(8,128)(2,1)S(1)}, u32[]{:S(2)}, u32[]{:S(2)}) %all-to-all-start) | async-done | bytes 262176 | tf_op jit(solution)/shard_map/all_to_all | solution.py:526
  130.9 0.8 reverse_select_fusion.h_ref
  131.6 5.9 %project.1 = (f32[128,2048]{1,0:T(8,128)}, bf16[2,640,512]{2,1,0:T(8,128)(2,1)}, bf16[2,640,512]{2,1,0:T(8,128)(2,1)}) custom-call(bf16[2,8,64,128]{3,2,1,0:T(8,128)(2,1)} %reverse_select_fusion.h_ref, bf16[1024,2048]{1,0:T(8,128)(2,1)} %w_ref.1, bf16[128,2048]{1,0:T(8,128)(2,1)} %s_ref.1, f32[1,2048]{1,0:T(1,128)} %bitcast.209, ...), custom_call_target="tpu_custom_call" | custom-call | flops 5000000000 | tf_op jit(solution)/shard_map/project/pallas_call | solution.py:276
  139.1 15.7 %collective-permute-done.23.refs_12_ = bf16[320,2048]{1,0:T(8,128)(2,1)} collective-permute-done((bf16[320,2048]{1,0:T(8,128)(2,1)S(1)}, bf16[320,2048]{1,0:T(8,128)(2,1)}, u32[]{:S(2)}, u32[]{:S(2)}) %collective-permute-start.23) | collective-permute-done | bytes 1310752 | tf_op jit(solution)/shard_map/ppermute | solution.py:532
  154.8 1.0 collective-permute-start.27
  155.9 7.9 %all-to-all-start.3 = ((bf16[32,40,512]{2,1,0:T(8,128)(2,1)}), bf16[32,40,512]{2,1,0:T(8,128)(2,1)}, u32[]{:S(2)}, u32[]{:S(2)}) async-start(bf16[32,40,512]{2,1,0:T(8,128)(2,1)} %bitcast.196), calls=%async_computation.3 | async-start | bytes 2621440 | tf_op jit(solution)/shard_map/all_to_all | solution.py:553
  163.9 1.4 fusion.5
  165.3 19.0 %all-to-all-done.3 = bf16[32,40,512]{2,1,0:T(8,128)(2,1)} async-done(((bf16[32,40,512]{2,1,0:T(8,128)(2,1)}), bf16[32,40,512]{2,1,0:T(8,128)(2,1)}, u32[]{:S(2)}, u32[]{:S(2)}) %all-to-all-start.3) | async-done | bytes 1310752 | tf_op jit(solution)/shard_map/all_to_all | solution.py:553
  184.3 5.3 %all-to-all-start.1 = ((bf16[32,40,512]{2,1,0:T(8,128)(2,1)}), bf16[32,40,512]{2,1,0:T(8,128)(2,1)}, u32[]{:S(2)}, u32[]{:S(2)}) async-start(bf16[32,40,512]{2,1,0:T(8,128)(2,1)} %bitcast.195), calls=%async_computation.1 | async-start | bytes 2621440 | tf_op jit(solution)/shard_map/all_to_all | solution.py:553
  189.6 18.4 %expert.3 = bf16[2,640,512]{2,1,0:T(8,128)(2,1)} custom-call(bf16[2,640,512]{2,1,0:T(8,128)(2,1)} %bitcast.40.refs_0_, bf16[640,640]{1,0:T(8,128)(2,1)} %get-tuple-element.68.refs_1_, bf16[640,640]{1,0:T(8,128)(2,1)} %get-tuple-element.67.refs_2_, bf16[2048,640]{1,0:T(8,128)(2,1)} %bitcast.refs_3_, bf16[2048,640]{1,0:T(8,128)(2,1)} %bitcast.1.refs_4_, ...), custom_call_target="tpu_custom_call" | custom-call | flops 16000000000 | tf_op jit(solution)/shard_map/expert/pallas_call | solution.py:379
  208.0 0.9 all-to-all-done.1
  208.9 8.1 %all-to-all-start.4 = ((bf16[32,40,512]{2,1,0:T(8,128)(2,1)}), bf16[32,40,512]{2,1,0:T(8,128)(2,1)S(1)}, u32[]{:S(2)}, u32[]{:S(2)}) async-start(bf16[32,40,512]{2,1,0:T(8,128)(2,1)} %bitcast.198), calls=%async_computation.4 | async-start | bytes 2621440 | tf_op jit(solution)/shard_map/all_to_all | solution.py:553
  217.0 18.4 %expert.2 = bf16[2,640,512]{2,1,0:T(8,128)(2,1)} custom-call(bf16[2,640,512]{2,1,0:T(8,128)(2,1)} %bitcast.36.refs_0_, bf16[640,640]{1,0:T(8,128)(2,1)} %get-tuple-element.68.refs_1_, bf16[640,640]{1,0:T(8,128)(2,1)} %get-tuple-element.67.refs_2_, bf16[2048,640]{1,0:T(8,128)(2,1)} %bitcast.refs_3_, bf16[2048,640]{1,0:T(8,128)(2,1)} %bitcast.1.refs_4_, ...), custom_call_target="tpu_custom_call" | custom-call | flops 16000000000 | tf_op jit(solution)/shard_map/expert/pallas_call | solution.py:379
  235.8 8.9 %all-to-all-start.2 = ((bf16[32,40,512]{2,1,0:T(8,128)(2,1)}), bf16[32,40,512]{2,1,0:T(8,128)(2,1)S(1)}, u32[]{:S(2)}, u32[]{:S(2)}) async-start(bf16[32,40,512]{2,1,0:T(8,128)(2,1)} %bitcast.197), calls=%async_computation.2 | async-start | bytes 2621440 | tf_op jit(solution)/shard_map/all_to_all | solution.py:553
  244.8 1.0 fusion.1
  245.8 1.6 pad_maximum_fusion.refs_2_
  247.5 15.5 %all-to-all-done.2 = bf16[32,40,512]{2,1,0:T(8,128)(2,1)S(1)} async-done(((bf16[32,40,512]{2,1,0:T(8,128)(2,1)}), bf16[32,40,512]{2,1,0:T(8,128)(2,1)S(1)}, u32[]{:S(2)}, u32[]{:S(2)}) %all-to-all-start.2) | async-done | bytes 1310752 | tf_op jit(solution)/shard_map/all_to_all | solution.py:553
  263.0 1.1 copy-done.2
  264.1 5.9 %combine.1 = bf16[128,2048]{1,0:T(8,128)(2,1)} custom-call(bf16[2,640,512]{2,1,0:T(8,128)(2,1)} %bitcast.191, bf16[2,640,512]{2,1,0:T(8,128)(2,1)} %bitcast.190, bf16[4,256,1280]{2,1,0:T(8,128)(2,1)} %pad_maximum_fusion.refs_2_, f32[128,2048]{1,0:T(8,128)} %get-tuple-element.42.refs_3_), custom_call_target="tpu_custom_call" | custom-call | tf_op jit(solution)/shard_map/combine/pallas_call | solution.py:420
  (93 shorter events, 5.7 us)
Async XLA Ops:
  0.0 9.4 %copy-start.5 = (bf16[1024,128]{1,0:T(8,128)(2,1)S(1)}, bf16[1024,128]{1,0:T(8,128)(2,1)}, u32[]{:S(2)}) copy-start(bf16[1024,128]{1,0:T(8,128)(2,1)} %param.13) | copy-start | bytes 786436
  0.0 12.5 %copy-start.6 = (s32[128,2]{0,1:T(2,128)S(1)}, s32[128,2]{0,1:T(2,128)}, u32[]{:S(2)}) copy-start(s32[128,2]{0,1:T(2,128)} %param.21) | copy-start | bytes 3076
  2.9 16.2 %collective-permute-start.12 = (bf16[512,256]{1,0:T(8,128)(2,1)}, bf16[512,256]{1,0:T(8,128)(2,1)S(1)}, u32[]{:S(2)}, u32[]{:S(2)}) collective-permute-start(bf16[512,256]{1,0:T(8,128)(2,1)} %get-tuple-element.57), channel_id=1, source_target_pairs={{0,32},{8,40},{16,48},{24,56},{32,64},{40,72},{48,80},{56,88},{64,... | collective-permute-start | bytes 786440 | tf_op jit(solution)/shard_map/ppermute | solution.py:199
  4.6 14.6 %collective-permute-start.13 = (bf16[512,256]{1,0:T(8,128)(2,1)}, bf16[512,256]{1,0:T(8,128)(2,1)S(1)}, u32[]{:S(2)}, u32[]{:S(2)}) collective-permute-start(bf16[512,256]{1,0:T(8,128)(2,1)} %get-tuple-element.57), channel_id=1, source_target_pairs={{0,96},{8,104},{16,112},{24,120},{32,0},{40,8},{48,16},{56,24},{64... | collective-permute-start | bytes 786440 | tf_op jit(solution)/shard_map/ppermute | solution.py:199
  6.7 20.3 %collective-permute-start.4 = (bf16[512,256]{1,0:T(8,128)(2,1)}, bf16[512,256]{1,0:T(8,128)(2,1)S(1)}, u32[]{:S(2)}, u32[]{:S(2)}) collective-permute-start(bf16[512,256]{1,0:T(8,128)(2,1)} %get-tuple-element.60), channel_id=1, source_target_pairs={{0,8},{8,16},{16,24},{24,0},{32,40},{40,48},{48,56},{56,32},{64,72... | collective-permute-start | bytes 786440 | tf_op jit(solution)/shard_map/ppermute | solution.py:199
  7.9 19.2 %collective-permute-start.5 = (bf16[512,256]{1,0:T(8,128)(2,1)}, bf16[512,256]{1,0:T(8,128)(2,1)S(1)}, u32[]{:S(2)}, u32[]{:S(2)}) collective-permute-start(bf16[512,256]{1,0:T(8,128)(2,1)} %get-tuple-element.60), channel_id=1, source_target_pairs={{0,24},{8,0},{16,8},{24,16},{32,56},{40,32},{48,40},{56,48},{64,88... | collective-permute-start | bytes 786440 | tf_op jit(solution)/shard_map/ppermute | solution.py:199
  10.0 43.7 %collective-permute-start.3 = (bf16[512,128]{1,0:T(8,128)(2,1)}, bf16[512,128]{1,0:T(8,128)(2,1)S(1)}, u32[]{:S(2)}, u32[]{:S(2)}) collective-permute-start(bf16[512,128]{1,0:T(8,128)(2,1)} %bitcast.7), channel_id=1, source_target_pairs={{0,120},{8,112},{16,104},{24,96},{32,88},{40,80},{48,72},{56,64},{... | collective-permute-start | bytes 393224 | tf_op jit(solution)/shard_map/ppermute | solution.py:221
  18.3 35.4 %copy-start.8 = (pred[128]{0:T(512)(128)(4,1)S(1)}, pred[128]{0:T(512)(128)(4,1)}, u32[]{:S(2)}) copy-start(pred[128]{0:T(512)(128)(4,1)} %constant.146.clone.1) | copy-start | bytes 388
  19.1 5.1 %collective-permute-start.14 = (bf16[256,256]{1,0:T(8,128)(2,1)S(1)}, bf16[256,256]{1,0:T(8,128)(2,1)S(1)}, u32[]{:S(2)}, u32[]{:S(2)}) collective-permute-start(bf16[256,256]{1,0:T(8,128)(2,1)S(1)} %slice.108), channel_id=1, source_target_pairs={{0,32},{8,40},{16,48},{24,56},{32,64},{40,72},{48,80},{56,88},{64,... | collective-permute-start | bytes 393224 | tf_op jit(solution)/shard_map/ppermute | solution.py:200
  19.2 5.0 %collective-permute-start.15 = (bf16[256,256]{1,0:T(8,128)(2,1)S(1)}, bf16[256,256]{1,0:T(8,128)(2,1)S(1)}, u32[]{:S(2)}, u32[]{:S(2)}) collective-permute-start(bf16[256,256]{1,0:T(8,128)(2,1)S(1)} %slice.109), channel_id=1, source_target_pairs={{0,96},{8,104},{16,112},{24,120},{32,0},{40,8},{48,16},{56,24},{64... | collective-permute-start | bytes 393224 | tf_op jit(solution)/shard_map/ppermute | solution.py:200
  24.3 29.6 %collective-permute-start.16 = (bf16[2048,256]{1,0:T(8,128)(2,1)S(1)}, bf16[2048,256]{1,0:T(8,128)(2,1)S(1)}, u32[]{:S(2)}, u32[]{:S(2)}) collective-permute-start(bf16[2048,256]{1,0:T(8,128)(2,1)S(1)} %constant_dynamic-update-slice_fusion.7.refs_5_), channel_id=1, source_target_pairs={{0,8},{8,16},{16,24},{24,0},{32,40},{40,48},{48,56},{56,32},{64,72... | collective-permute-start | bytes 3145736 | tf_op jit(solution)/shard_map/ppermute | solution.py:199
  24.3 29.7 %collective-permute-start.18 = (bf16[2048,256]{1,0:T(8,128)(2,1)S(1)}, bf16[2048,256]{1,0:T(8,128)(2,1)S(1)}, u32[]{:S(2)}, u32[]{:S(2)}) collective-permute-start(bf16[2048,256]{1,0:T(8,128)(2,1)S(1)} %constant_dynamic-update-slice_fusion.7.refs_5_), channel_id=1, source_target_pairs={{0,24},{8,0},{16,8},{24,16},{32,56},{40,32},{48,40},{56,48},{64,88... | collective-permute-start | bytes 3145736 | tf_op jit(solution)/shard_map/ppermute | solution.py:199
  27.0 22.8 %collective-permute-start.6 = (bf16[256,256]{1,0:T(8,128)(2,1)S(1)}, bf16[256,256]{1,0:T(8,128)(2,1)S(1)}, u32[]{:S(2)}, u32[]{:S(2)}) collective-permute-start(bf16[256,256]{1,0:T(8,128)(2,1)S(1)} %slice.103), channel_id=1, source_target_pairs={{0,8},{8,16},{16,24},{24,0},{32,40},{40,48},{48,56},{56,32},{64,72... | collective-permute-start | bytes 393224 | tf_op jit(solution)/shard_map/ppermute | solution.py:200
  27.2 24.0 %collective-permute-start.7 = (bf16[256,256]{1,0:T(8,128)(2,1)S(1)}, bf16[256,256]{1,0:T(8,128)(2,1)S(1)}, u32[]{:S(2)}, u32[]{:S(2)}) collective-permute-start(bf16[256,256]{1,0:T(8,128)(2,1)S(1)} %slice.104), channel_id=1, source_target_pairs={{0,24},{8,0},{16,8},{24,16},{32,56},{40,32},{48,40},{56,48},{64,88... | collective-permute-start | bytes 393224 | tf_op jit(solution)/shard_map/ppermute | solution.py:200
  29.9 26.9 %copy-start = (f32[128]{0:T(128)S(1)}, f32[128]{0:T(128)}, u32[]{:S(2)}) copy-start(f32[128]{0:T(128)} %param.17) | copy-start | bytes 1540
  49.8 88.1 %collective-permute-start = (bf16[2048,640]{1,0:T(8,128)(2,1)}, bf16[2048,640]{1,0:T(8,128)(2,1)}, u32[]{:S(2)}, u32[]{:S(2)}) collective-permute-start(bf16[2048,640]{1,0:T(8,128)(2,1)} %bitcast.refs_3_), channel_id=1, source_target_pairs={{0,6},{1,3},{2,0},{3,5},{4,2},{5,7},{6,4},{7,1},{8,14},{9,11},{10,... | collective-permute-start | bytes 7864328 | tf_op jit(solution)/shard_map/ppermute | solution.py:469
  51.2 21.7 %collective-permute-start.10 = (bf16[2048,256]{1,0:T(8,128)(2,1)S(1)}, bf16[2048,256]{1,0:T(8,128)(2,1)S(1)}, u32[]{:S(2)}, u32[]{:S(2)}) collective-permute-start(bf16[2048,256]{1,0:T(8,128)(2,1)S(1)} %constant_dynamic-update-slice_fusion.2.refs_4_), channel_id=1, source_target_pairs={{0,96},{8,104},{16,112},{24,120},{32,0},{40,8},{48,16},{56,24},{64... | collective-permute-start | bytes 3145736 | tf_op jit(solution)/shard_map/ppermute | solution.py:199
  53.7 22.1 %collective-permute-start.8 = (bf16[2048,256]{1,0:T(8,128)(2,1)S(1)}, bf16[2048,256]{1,0:T(8,128)(2,1)S(1)}, u32[]{:S(2)}, u32[]{:S(2)}) collective-permute-start(bf16[2048,256]{1,0:T(8,128)(2,1)S(1)} %constant_dynamic-update-slice_fusion.2.refs_4_), channel_id=1, source_target_pairs={{0,32},{8,40},{16,48},{24,56},{32,64},{40,72},{48,80},{56,88},{64,... | collective-permute-start | bytes 3145736 | tf_op jit(solution)/shard_map/ppermute | solution.py:199
  54.0 26.6 %collective-permute-start.17 = (bf16[1024,256]{1,0:T(8,128)(2,1)S(1)}, bf16[1024,256]{1,0:T(8,128)(2,1)S(1)}, u32[]{:S(2)}, u32[]{:S(2)}) collective-permute-start(bf16[1024,256]{1,0:T(8,128)(2,1)S(1)} %slice.110), channel_id=1, source_target_pairs={{0,8},{8,16},{16,24},{24,0},{32,40},{40,48},{48,56},{56,32},{64,72... | collective-permute-start | bytes 1572872 | tf_op jit(solution)/shard_map/ppermute | solution.py:200
  54.1 27.1 %collective-permute-start.19 = (bf16[1024,256]{1,0:T(8,128)(2,1)S(1)}, bf16[1024,256]{1,0:T(8,128)(2,1)S(1)}, u32[]{:S(2)}, u32[]{:S(2)}) collective-permute-start(bf16[1024,256]{1,0:T(8,128)(2,1)S(1)} %slice.111), channel_id=1, source_target_pairs={{0,24},{8,0},{16,8},{24,16},{32,56},{40,32},{48,40},{56,48},{64,88... | collective-permute-start | bytes 1572872 | tf_op jit(solution)/shard_map/ppermute | solution.py:200
  72.8 65.6 %collective-permute-start.1 = (bf16[2048,640]{1,0:T(8,128)(2,1)}, bf16[2048,640]{1,0:T(8,128)(2,1)}, u32[]{:S(2)}, u32[]{:S(2)}) collective-permute-start(bf16[2048,640]{1,0:T(8,128)(2,1)} %bitcast.1.refs_4_), channel_id=1, source_target_pairs={{0,6},{1,3},{2,0},{3,5},{4,2},{5,7},{6,4},{7,1},{8,14},{9,11},{10,... | collective-permute-start | bytes 7864328 | tf_op jit(solution)/shard_map/ppermute | solution.py:469
  75.8 62.7 %collective-permute-start.20 = (bf16[2048,640]{1,0:T(8,128)(2,1)}, bf16[2048,640]{1,0:T(8,128)(2,1)}, u32[]{:S(2)}, u32[]{:S(2)}) collective-permute-start(bf16[2048,640]{1,0:T(8,128)(2,1)} %bitcast.refs_3_), channel_id=1, source_target_pairs={{0,1},{1,0},{2,3},{3,2},{4,5},{5,4},{6,7},{7,6},{8,9},{9,8},{10,11... | collective-permute-start | bytes 7864328 | tf_op jit(solution)/shard_map/ppermute | solution.py:518
  80.5 16.7 %collective-permute-start.11 = (bf16[1024,256]{1,0:T(8,128)(2,1)S(1)}, bf16[1024,256]{1,0:T(8,128)(2,1)S(1)}, u32[]{:S(2)}, u32[]{:S(2)}) collective-permute-start(bf16[1024,256]{1,0:T(8,128)(2,1)S(1)} %slice.106), channel_id=1, source_target_pairs={{0,96},{8,104},{16,112},{24,120},{32,0},{40,8},{48,16},{56,24},{64... | collective-permute-start | bytes 1572872 | tf_op jit(solution)/shard_map/ppermute | solution.py:200
  81.2 17.1 %collective-permute-start.9 = (bf16[1024,256]{1,0:T(8,128)(2,1)S(1)}, bf16[1024,256]{1,0:T(8,128)(2,1)S(1)}, u32[]{:S(2)}, u32[]{:S(2)}) collective-permute-start(bf16[1024,256]{1,0:T(8,128)(2,1)S(1)} %slice.105), channel_id=1, source_target_pairs={{0,32},{8,40},{16,48},{24,56},{32,64},{40,72},{48,80},{56,88},{64,... | collective-permute-start | bytes 1572872 | tf_op jit(solution)/shard_map/ppermute | solution.py:200
  97.2 40.3 %collective-permute-start.2 = (bf16[320,2048]{1,0:T(8,128)(2,1)}, bf16[320,2048]{1,0:T(8,128)(2,1)}, u32[]{:S(2)}, u32[]{:S(2)}) collective-permute-start(bf16[320,2048]{1,0:T(8,128)(2,1)} %get-tuple-element.56), channel_id=1, source_target_pairs={{0,6},{1,3},{2,0},{3,5},{4,2},{5,7},{6,4},{7,1},{8,14},{9,11},{10,... | collective-permute-start | bytes 3932168 | tf_op jit(solution)/shard_map/ppermute | solution.py:469
  98.3 40.6 %collective-permute-start.21 = (bf16[2048,640]{1,0:T(8,128)(2,1)}, bf16[2048,640]{1,0:T(8,128)(2,1)}, u32[]{:S(2)}, u32[]{:S(2)}) collective-permute-start(bf16[2048,640]{1,0:T(8,128)(2,1)} %bitcast.1.refs_4_), channel_id=1, source_target_pairs={{0,1},{1,0},{2,3},{3,2},{4,5},{5,4},{6,7},{7,6},{8,9},{9,8},{10,11... | collective-permute-start | bytes 7864328 | tf_op jit(solution)/shard_map/ppermute | solution.py:518
  105.9 25.0 %all-to-all-start = ((bf16[16,64,128]{2,1,0:T(8,128)(2,1)}), bf16[16,64,128]{2,1,0:T(8,128)(2,1)S(1)}, u32[]{:S(2)}, u32[]{:S(2)}) async-start(bf16[16,64,128]{2,1,0:T(8,128)(2,1)} %bitcast.14), calls=%async_computation | async-start | bytes 524288 | tf_op jit(solution)/shard_map/all_to_all | solution.py:526
  131.6 5.9 %copy-start.3 = (bf16[1,640,2048]{2,1,0:T(8,128)(2,1)S(1)}, bf16[1,640,2048]{2,1,0:T(8,128)(2,1)}, u32[]{:S(2)}) copy-start(bf16[1,640,2048]{2,1,0:T(8,128)(2,1)} %param.25) | copy-start | bytes 7864324
  131.6 6.3 %copy-start.4 = (bf16[320,2048]{1,0:T(8,128)(2,1)S(1)}, bf16[320,2048]{1,0:T(8,128)(2,1)}, u32[]{:S(2)}) copy-start(bf16[320,2048]{1,0:T(8,128)(2,1)} %get-tuple-element.40) | copy-start | bytes 3932164
  137.5 52.0 %collective-permute-start.22 = (bf16[640,2048]{1,0:T(8,128)(2,1)S(1)}, bf16[640,2048]{1,0:T(8,128)(2,1)}, u32[]{:S(2)}, u32[]{:S(2)}) collective-permute-start(bf16[640,2048]{1,0:T(8,128)(2,1)S(1)} %bitcast.194), channel_id=1, source_target_pairs={{0,1},{1,0},{2,3},{3,2},{4,5},{5,4},{6,7},{7,6},{8,9},{9,8},{10,11... | collective-permute-start | bytes 7864328 | tf_op jit(solution)/shard_map/ppermute | solution.py:518
  138.0 16.9 %collective-permute-start.23 = (bf16[320,2048]{1,0:T(8,128)(2,1)S(1)}, bf16[320,2048]{1,0:T(8,128)(2,1)}, u32[]{:S(2)}, u32[]{:S(2)}) collective-permute-start(bf16[320,2048]{1,0:T(8,128)(2,1)S(1)} %copy-done.4), channel_id=1, source_target_pairs={{0,6},{1,3},{2,0},{3,5},{4,2},{5,7},{6,4},{7,1},{8,14},{9,11},{10,... | collective-permute-start | bytes 3932168 | tf_op jit(solution)/shard_map/ppermute | solution.py:532
  138.4 51.2 %collective-permute-start.24 = (bf16[2048,640]{1,0:T(8,128)(2,1)}, bf16[2048,640]{1,0:T(8,128)(2,1)}, u32[]{:S(2)}, u32[]{:S(2)}) collective-permute-start(bf16[2048,640]{1,0:T(8,128)(2,1)} %collective-permute-done.refs_9_), channel_id=1, source_target_pairs={{0,1},{1,0},{2,3},{3,2},{4,5},{5,4},{6,7},{7,6},{8,9},{9,8},{10,11... | collective-permute-start | bytes 7864328 | tf_op jit(solution)/shard_map/ppermute | solution.py:536
  138.6 51.0 %collective-permute-start.25 = (bf16[2048,640]{1,0:T(8,128)(2,1)}, bf16[2048,640]{1,0:T(8,128)(2,1)}, u32[]{:S(2)}, u32[]{:S(2)}) collective-permute-start(bf16[2048,640]{1,0:T(8,128)(2,1)} %collective-permute-done.1.refs_10_), channel_id=1, source_target_pairs={{0,1},{1,0},{2,3},{3,2},{4,5},{5,4},{6,7},{7,6},{8,9},{9,8},{10,11... | collective-permute-start | bytes 7864328 | tf_op jit(solution)/shard_map/ppermute | solution.py:536
  138.9 50.6 %collective-permute-start.26 = (bf16[320,2048]{1,0:T(8,128)(2,1)}, bf16[320,2048]{1,0:T(8,128)(2,1)}, u32[]{:S(2)}, u32[]{:S(2)}) collective-permute-start(bf16[320,2048]{1,0:T(8,128)(2,1)} %collective-permute-done.2.refs_11_), channel_id=1, source_target_pairs={{0,1},{1,0},{2,3},{3,2},{4,5},{5,4},{6,7},{7,6},{8,9},{9,8},{10,11... | collective-permute-start | bytes 3932168 | tf_op jit(solution)/shard_map/ppermute | solution.py:536
  154.8 34.8 %collective-permute-start.27 = (bf16[320,2048]{1,0:T(8,128)(2,1)}, bf16[320,2048]{1,0:T(8,128)(2,1)}, u32[]{:S(2)}, u32[]{:S(2)}) collective-permute-start(bf16[320,2048]{1,0:T(8,128)(2,1)} %collective-permute-done.23.refs_12_), channel_id=1, source_target_pairs={{0,1},{1,0},{2,3},{3,2},{4,5},{5,4},{6,7},{7,6},{8,9},{9,8},{10,11... | collective-permute-start | bytes 3932168 | tf_op jit(solution)/shard_map/ppermute | solution.py:537
  155.9 28.4 %all-to-all-start.3 = ((bf16[32,40,512]{2,1,0:T(8,128)(2,1)}), bf16[32,40,512]{2,1,0:T(8,128)(2,1)}, u32[]{:S(2)}, u32[]{:S(2)}) async-start(bf16[32,40,512]{2,1,0:T(8,128)(2,1)} %bitcast.196), calls=%async_computation.3 | async-start | bytes 2621440 | tf_op jit(solution)/shard_map/all_to_all | solution.py:553
  184.3 24.6 %all-to-all-start.1 = ((bf16[32,40,512]{2,1,0:T(8,128)(2,1)}), bf16[32,40,512]{2,1,0:T(8,128)(2,1)}, u32[]{:S(2)}, u32[]{:S(2)}) async-start(bf16[32,40,512]{2,1,0:T(8,128)(2,1)} %bitcast.195), calls=%async_computation.1 | async-start | bytes 2621440 | tf_op jit(solution)/shard_map/all_to_all | solution.py:553
  208.9 26.9 %all-to-all-start.4 = ((bf16[32,40,512]{2,1,0:T(8,128)(2,1)}), bf16[32,40,512]{2,1,0:T(8,128)(2,1)S(1)}, u32[]{:S(2)}, u32[]{:S(2)}) async-start(bf16[32,40,512]{2,1,0:T(8,128)(2,1)} %bitcast.198), calls=%async_computation.4 | async-start | bytes 2621440 | tf_op jit(solution)/shard_map/all_to_all | solution.py:553
  235.4 9.4 %copy-start.7 = (f32[128,2]{0,1:T(2,128)S(1)}, f32[128,2]{0,1:T(2,128)}, u32[]{:S(2)}) copy-start(f32[128,2]{0,1:T(2,128)} %param.22) | copy-start | bytes 3076
  235.8 10.0 %copy-start.1 = (bf16[32,40,512]{2,1,0:T(8,128)(2,1)}, bf16[32,40,512]{2,1,0:T(8,128)(2,1)S(1)}, u32[]{:S(2)}) copy-start(bf16[32,40,512]{2,1,0:T(8,128)(2,1)S(1)} %all-to-all-done.4) | copy-start | bytes 3932164
  235.8 27.2 %all-to-all-start.2 = ((bf16[32,40,512]{2,1,0:T(8,128)(2,1)}), bf16[32,40,512]{2,1,0:T(8,128)(2,1)S(1)}, u32[]{:S(2)}, u32[]{:S(2)}) async-start(bf16[32,40,512]{2,1,0:T(8,128)(2,1)} %bitcast.197), calls=%async_computation.2 | async-start | bytes 2621440 | tf_op jit(solution)/shard_map/all_to_all | solution.py:553
  263.0 1.1 copy-start.2

commit v2 on v1

--- a/solution.py
+++ b/solution.py
@@ -122,11 +122,11 @@
             run([(m, r) for r in range(rows // ROWS) for m in range(2)])
         else:
 
-            def some(t, carry):
-                run([(t % 2, t // 2)])
+            def some(r, carry):
+                run([(m, r) for m in range(2)])
                 return carry
 
-            lax.fori_loop(0, 2 * rows // ROWS, some, 0)
+            lax.fori_loop(0, rows // ROWS, some, 0)
 
     def half(h, carry):
         number = bounds[h]
@@ -201,7 +201,7 @@
     return (before, behind), far
 
 
-def attend(queries, key_rows, value_rows, lambdas, head_gain, weights, swap):
+def attend(queries, key_rows, value_rows, lambdas, head_gain, weights, later):
     sp_size, tp_size = lax.axis_size("sp"), lax.axis_size("tp")
     side = math.isqrt(sp_size)
     sp = lax.axis_index("sp")
@@ -247,8 +247,8 @@
         )
         if n == 0:
             weights, state = lax.optimization_barrier((weights, state))
-            swapped = tuple(swap(w) for w in weights)
-    return state, swapped
+            moved_late = later(weights)
+    return state, moved_late
 
 
 def project_body(h_ref, w_ref, s_ref, g_ref, d_ref, a_ref, *o_refs):
@@ -399,6 +399,28 @@
     )(arrived, select, place, *flat)
 
 
+def halves_body(w_any, a_any, b_any, sem):
+    rows = a_any.shape[0]
+    first = pltpu.make_async_copy(w_any.at[pl.ds(0, rows)], a_any, sem.at[0])
+    second = pltpu.make_async_copy(w_any.at[pl.ds(rows, rows)], b_any, sem.at[1])
+    first.start()
+    second.start()
+    first.wait()
+    second.wait()
+
+
+def halves(w):
+    out = jax.ShapeDtypeStruct((w.shape[0] // 2, w.shape[1]), w.dtype)
+    return pl.pallas_call(
+        halves_body,
+        in_specs=[pl.BlockSpec(memory_space=pl.ANY)],
+        out_specs=[pl.BlockSpec(memory_space=pltpu.HBM)] * 2,
+        out_shape=[out, out],
+        scratch_shapes=[pltpu.SemaphoreType.DMA((2,))],
+        name="halves",
+    )(w)
+
+
 def combine_body(*refs):
     r_refs, (w_ref, a_ref, o_ref, r_sc) = refs[:CHUNKS], refs[CHUNKS:]
     wide = r_refs[0].shape[2]
@@ -463,11 +485,14 @@
     along = moved(sp_size, tp_size, lambda c: 2 * c - 1, 0)
     sibling = moved(sp_size, tp_size, lambda c: 0, 1)
     passed = []
-    gate, up, down = mine
-    later = down.shape[0] // 2
-    for w in (gate, up, down[:later]):
+    passed = []
+    for w in mine[:2]:
         passed.append(lax.ppermute(w, BOTH, along))
-    passed = tuple(passed)
+
+    def later(weights):
+        soon, rest = halves(weights[2])
+        soon = lax.ppermute(soon, BOTH, along)
+        return tuple(lax.ppermute(w, BOTH, sibling) for w in weights), soon, rest
 
     slots = max(2, (rows_local * top_count * 5 + 4 * experts - 1) // (4 * experts))
     part = slots // CHUNKS
@@ -514,9 +539,10 @@
     select = (cuts[:, None] == places).astype(BF16)
     place = (places[:, None] == cuts).astype(BF16)
 
-    heads, mine_too = attend(
-        queries, key_rows, value_rows, lambdas, head_gain, mine, lambda w: lax.ppermute(w, BOTH, sibling)
-    )
+    heads, (mine_too, soon, rest) = attend(
+        queries, key_rows, value_rows, lambdas, head_gain, mine, later
+    )
+    passed = tuple(passed) + (soon,)
     half = rows_local // 2
     heads = heads.reshape(2 * tp_size, half, 128)
     groups = [
@@ -528,7 +554,7 @@
     ).reshape(2, tp_size, half, 128)
     heads = jnp.where(low, heads, heads[::-1])
 
-    rest, heads = lax.optimization_barrier((down[later:], heads))
+    rest, heads = lax.optimization_barrier((rest, heads))
     rest = lax.ppermute(rest, BOTH, along)
     attended, *outgoing = project(heads, out_weight, stream, ffn_gain, dispatch)
 

time: 274 us -> 348 us (1.27)
  Pallas kernels: 81.3 us -> 161 us
  waiting for transfers between devices: 94.9 us -> 82.5 us
  local copies, waits for them, and re-layouts: 10.6 us -> 19.3 us
    pallas_call x0 -> x1, Pallas kernels: none -> 80.5 us  [halves(): pl.pallas_call(halves_body, in_specs=[pl.BlockSpec(memory_space=pl.ANY)],...]
    unnamed x28 -> x38, local copies, waits for them, and re-layouts: 3.35 us -> 11.8 us
    ppermute x4, waiting for transfers between devices: 5.92 us -> 0.01 us  [spread(): lax.ppermute(array, 'sp', back)]
    all_to_all x1, waiting for transfers between devices: 13 us -> 7.63 us  [local(): lax.all_to_all(heads, BOTH, split_axis=0, concat_axis=0, tiled=True, axis...]
    slice x1 -> x0, local copies, waits for them, and re-layouts: 3.6 us -> none  [local(): rest, heads = lax.optimization_barrier((down[later:], heads))]
  transfers between devices with their start and end apart: 33 -> 33, of which waited for: 10 -> 8; matrix products, arithmetic and copies ran while one was open for 5% -> 5% of each run, Pallas kernels for 28% -> 45%
where the time goes in v2:
time: 348 us; the launch traced here: 344 us
  Pallas kernels  161 us (46%)
  waiting for transfers between devices  82.5 us (24%)
  starting transfers between devices  73.4 us (21%)
  local copies, waits for them, and re-layouts  19.3 us (6%)
  other arithmetic  7.16 us (2%)
    pallas_call x1, Pallas kernels, halves(): pl.pallas_call(halves_body, in_specs=[pl.BlockSpec(memory_space=pl.ANY)],...  80.5 us
    pallas_call x2, Pallas kernels, expert(): pl.pallas_call(lambda *refs: expert_body([len(one) for one in sets], *ref...  36.8 us
    all_to_all x4, waiting for transfers between devices, exchange(): lax.all_to_all(x, BOTH, split_axis=0, concat_axis=0, tiled=True, axis_ind...  36.1 us
    pallas_call x3, Pallas kernels, attention(): pl.pallas_call(lambda *refs: attention_body(pieces, side, first, final, l...  31.6 us
    all_to_all x4, starting transfers between devices, exchange(): lax.all_to_all(x, BOTH, split_axis=0, concat_axis=0, tiled=True, axis_ind...  29.1 us
    ppermute x4, waiting for transfers between devices, spread(): lax.ppermute(before[:half], 'sp', forth)  24.2 us
    ppermute x1, waiting for transfers between devices, local(): rest = lax.ppermute(rest, BOTH, along)  14.5 us
    unnamed x38, local copies, waits for them, and re-layouts  11.8 us
  transfers between devices with their start and end apart: 33, of which 8 were waited for; matrix products, arithmetic and copies ran while one was open for 5% of the time, Pallas kernels for 45%

profile of v2, /device:TPU:9, one launch (start us, length us, event | category | flops | bytes accessed | tf_op | source)
XLA Modules:
  0.0 344.4 jit_solution(15521516409212625327)
XLA Ops:
  0.0 1.0 constant_dynamic-update-slice_fusion.1
  1.0 1.0 constant_dynamic-update-slice_fusion
  3.0 1.6 collective-permute-start.7
  4.6 2.1 collective-permute-start.8
  6.7 1.2 collective-permute-start.3
  7.9 1.5 collective-permute-start.4
  9.4 2.5 collective-permute-start.2
  13.7 2.7 collective-permute-start.10
  17.9 3.5 %collective-permute-done.9 = bf16[256,256]{1,0:T(8,128)(2,1)S(1)} collective-permute-done((bf16[256,256]{1,0:T(8,128)(2,1)S(1)}, bf16[256,256]{1,0:T(8,128)(2,1)S(1)}, u32[]{:S(2)}, u32[]{:S(2)}) %collective-permute-start.9) | collective-permute-done | bytes 131104 | tf_op jit(solution)/shard_map/ppermute | solution.py:200
  22.8 2.7 collective-permute-start.18
  25.6 2.7 collective-permute-start.6
  29.8 20.7 %collective-permute-done.5 = bf16[256,256]{1,0:T(8,128)(2,1)S(1)} collective-permute-done((bf16[256,256]{1,0:T(8,128)(2,1)S(1)}, bf16[256,256]{1,0:T(8,128)(2,1)S(1)}, u32[]{:S(2)}, u32[]{:S(2)}) %collective-permute-start.5) | collective-permute-done | bytes 131104 | tf_op jit(solution)/shard_map/ppermute | solution.py:200
  50.5 1.3 collective-permute-start
  53.1 2.7 collective-permute-start.14
  57.7 2.7 collective-permute-start.19
  60.4 9.5 %attention.3 = (f32[2,2,512,128]{3,2,1,0:T(8,128)S(1)}, f32[2,2,512,256]{3,2,1,0:T(8,128)S(1)}) custom-call(s32[1]{0:T(128)} %bitcast.3.refs_0_, f32[1]{0:T(128)S(6)} %copy.72.refs_1_, f32[1,128]{1,0:T(1,128)S(1)} %bitcast.183, bf16[2,2,512,128]{3,2,1,0:T(8,128)(2,1)S(1)} %pad_maximum_fusion.1.refs_3_, ...), custom_call_target="tpu_custom_call" | custom-call | flops 8000000000 | tf_op jit(solution)/shard_map/attention/pallas_call | solution.py:183
  69.8 1.4 copy-done.1
  71.2 1.0 copy-done.3
  72.2 80.5 %halves.1 = (bf16[320,2048]{1,0:T(8,128)(2,1)}, bf16[320,2048]{1,0:T(8,128)(2,1)}) custom-call(bf16[640,2048]{1,0:T(8,128)(2,1)} %bitcast.188), custom_call_target="tpu_custom_call" | custom-call | tf_op jit(solution)/shard_map/halves/pallas_call | solution.py:414
  152.8 1.1 collective-permute-start.1
  153.8 1.1 slice.92
  154.9 4.5 %collective-permute-start.22 = (bf16[640,2048]{1,0:T(8,128)(2,1)}, bf16[640,2048]{1,0:T(8,128)(2,1)}, u32[]{:S(2)}, u32[]{:S(2)}) collective-permute-start(bf16[640,2048]{1,0:T(8,128)(2,1)} %bitcast.189), channel_id=1, source_target_pairs={{0,1},{1,0},{2,3},{3,2},{4,5},{5,4},{6,7},{7,6},{8,9},{9,8},{10,11... | collective-permute-start | bytes 7864328 | tf_op jit(solution)/shard_map/ppermute | solution.py:495
  159.4 1.1 slice.93
  160.6 2.7 collective-permute-start.15
  163.2 1.6 copy-done.2
  164.8 1.2 copy-done.4
  166.0 13.9 %attention.4 = (f32[2,2,512,128]{3,2,1,0:T(8,128)S(1)}, f32[2,2,512,256]{3,2,1,0:T(8,128)S(1)}) custom-call(s32[1]{0:T(128)} %bitcast.3.refs_0_, f32[1]{0:T(128)S(6)} %copy.72.refs_1_, f32[1,128]{1,0:T(1,128)S(1)} %bitcast.184, bf16[2,2,512,128]{3,2,1,0:T(8,128)(2,1)S(1)} %pad_maximum_fusion.1.refs_3_, bf16[2048,256]{1,0:T(8,128)(2,1)} %collective-permute-done.12.refs_4_, ...), custom_call_target="tpu_custom_call" | custom-call | flops 16000000000 | tf_op jit(solution)/shard_map/attention/pallas_call | solution.py:183
  180.1 1.3 collective-permute-start.20
  181.4 8.2 %attention.5 = bf16[2,512,128]{2,1,0:T(8,128)(2,1)} custom-call(s32[1]{0:T(128)} %bitcast.3.refs_0_, f32[1]{0:T(128)S(6)} %copy.72.refs_1_, f32[1,128]{1,0:T(1,128)S(1)} %bitcast.185, bf16[2,2,512,128]{3,2,1,0:T(8,128)(2,1)S(1)} %pad_maximum_fusion.1.refs_3_, bf16[1024,256]{1,0:T(8,128)(2,1)S(1)} %collective-permute-done.13.refs_4_, ...), custom_call_target="tpu_custom_call" | custom-call | flops 8000000000 | tf_op jit(solution)/shard_map/attention/pallas_call | solution.py:183
  189.6 7.1 %all-to-all-start = ((bf16[16,64,128]{2,1,0:T(8,128)(2,1)}), bf16[16,64,128]{2,1,0:T(8,128)(2,1)S(1)}, u32[]{:S(2)}, u32[]{:S(2)}) async-start(bf16[16,64,128]{2,1,0:T(8,128)(2,1)} %bitcast.12), calls=%async_computation | async-start | bytes 524288 | tf_op jit(solution)/shard_map/all_to_all | solution.py:552
  196.7 1.9 fusion.6.d_ref
  198.6 7.6 %all-to-all-done = bf16[16,64,128]{2,1,0:T(8,128)(2,1)S(1)} async-done(((bf16[16,64,128]{2,1,0:T(8,128)(2,1)}), bf16[16,64,128]{2,1,0:T(8,128)(2,1)S(1)}, u32[]{:S(2)}, u32[]{:S(2)}) %all-to-all-start) | async-done | bytes 262176 | tf_op jit(solution)/shard_map/all_to_all | solution.py:552
  207.0 5.8 %project.1 = (f32[128,2048]{1,0:T(8,128)}, bf16[2,640,512]{2,1,0:T(8,128)(2,1)}, bf16[2,640,512]{2,1,0:T(8,128)(2,1)}) custom-call(bf16[2,8,64,128]{3,2,1,0:T(8,128)(2,1)} %reverse_select_fusion.h_ref, bf16[1024,2048]{1,0:T(8,128)(2,1)} %w_ref.1, bf16[128,2048]{1,0:T(8,128)(2,1)} %s_ref.1, f32[1,2048]{1,0:T(1,128)} %bitcast.208, ...), custom_call_target="tpu_custom_call" | custom-call | flops 5000000000 | tf_op jit(solution)/shard_map/project/pallas_call | solution.py:276
  213.6 1.8 collective-permute-start.24
  215.9 14.5 %collective-permute-done.23.refs_12_ = bf16[320,2048]{1,0:T(8,128)(2,1)} collective-permute-done((bf16[320,2048]{1,0:T(8,128)(2,1)S(1)}, bf16[320,2048]{1,0:T(8,128)(2,1)}, u32[]{:S(2)}, u32[]{:S(2)}) %collective-permute-start.23) | collective-permute-done | bytes 1310752 | tf_op jit(solution)/shard_map/ppermute | solution.py:558
  231.1 7.2 %all-to-all-start.3 = ((bf16[32,40,512]{2,1,0:T(8,128)(2,1)}), bf16[32,40,512]{2,1,0:T(8,128)(2,1)S(1)}, u32[]{:S(2)}, u32[]{:S(2)}) async-start(bf16[32,40,512]{2,1,0:T(8,128)(2,1)} %bitcast.192), calls=%async_computation.3 | async-start | bytes 2621440 | tf_op jit(solution)/shard_map/all_to_all | solution.py:579
  238.4 1.4 fusion.5
  239.8 18.9 %all-to-all-done.3 = bf16[32,40,512]{2,1,0:T(8,128)(2,1)S(1)} async-done(((bf16[32,40,512]{2,1,0:T(8,128)(2,1)}), bf16[32,40,512]{2,1,0:T(8,128)(2,1)S(1)}, u32[]{:S(2)}, u32[]{:S(2)}) %all-to-all-start.3) | async-done | bytes 1310752 | tf_op jit(solution)/shard_map/all_to_all | solution.py:579
  258.8 4.9 %all-to-all-start.1 = ((bf16[32,40,512]{2,1,0:T(8,128)(2,1)}), bf16[32,40,512]{2,1,0:T(8,128)(2,1)S(1)}, u32[]{:S(2)}, u32[]{:S(2)}) async-start(bf16[32,40,512]{2,1,0:T(8,128)(2,1)} %bitcast.33), calls=%async_computation.1 | async-start | bytes 2621440 | tf_op jit(solution)/shard_map/all_to_all | solution.py:579
  263.8 18.4 %expert.3 = bf16[2,640,512]{2,1,0:T(8,128)(2,1)} custom-call(bf16[2,640,512]{2,1,0:T(8,128)(2,1)} %bitcast.194, bf16[640,640]{1,0:T(8,128)(2,1)} %get-tuple-element.70.refs_1_, bf16[640,640]{1,0:T(8,128)(2,1)} %get-tuple-element.69.refs_2_, bf16[2048,640]{1,0:T(8,128)(2,1)} %bitcast.refs_3_, bf16[2048,640]{1,0:T(8,128)(2,1)} %bitcast.1.refs_4_, ...), custom_call_target="tpu_custom_call" | custom-call | flops 16000000000 | tf_op jit(solution)/shard_map/expert/pallas_call | solution.py:379
  282.2 1.1 all-to-all-done.1
  283.3 8.2 %all-to-all-start.4 = ((bf16[32,40,512]{2,1,0:T(8,128)(2,1)}), bf16[32,40,512]{2,1,0:T(8,128)(2,1)S(1)}, u32[]{:S(2)}, u32[]{:S(2)}) async-start(bf16[32,40,512]{2,1,0:T(8,128)(2,1)} %bitcast.196), calls=%async_computation.4 | async-start | bytes 2621440 | tf_op jit(solution)/shard_map/all_to_all | solution.py:579
  291.5 18.3 %expert.2 = bf16[2,640,512]{2,1,0:T(8,128)(2,1)} custom-call(bf16[2,640,512]{2,1,0:T(8,128)(2,1)} %bitcast.195, bf16[640,640]{1,0:T(8,128)(2,1)} %get-tuple-element.70.refs_1_, bf16[640,640]{1,0:T(8,128)(2,1)} %get-tuple-element.69.refs_2_, bf16[2048,640]{1,0:T(8,128)(2,1)} %bitcast.refs_3_, bf16[2048,640]{1,0:T(8,128)(2,1)} %bitcast.1.refs_4_, ...), custom_call_target="tpu_custom_call" | custom-call | flops 16000000000 | tf_op jit(solution)/shard_map/expert/pallas_call | solution.py:379
  310.3 8.8 %all-to-all-start.2 = ((bf16[32,40,512]{2,1,0:T(8,128)(2,1)}), bf16[32,40,512]{2,1,0:T(8,128)(2,1)S(1)}, u32[]{:S(2)}, u32[]{:S(2)}) async-start(bf16[32,40,512]{2,1,0:T(8,128)(2,1)} %bitcast.193), calls=%async_computation.2 | async-start | bytes 2621440 | tf_op jit(solution)/shard_map/all_to_all | solution.py:579
  320.2 1.6 pad_maximum_fusion.refs_2_
  321.9 15.6 %all-to-all-done.2 = bf16[32,40,512]{2,1,0:T(8,128)(2,1)S(1)} async-done(((bf16[32,40,512]{2,1,0:T(8,128)(2,1)}), bf16[32,40,512]{2,1,0:T(8,128)(2,1)S(1)}, u32[]{:S(2)}, u32[]{:S(2)}) %all-to-all-start.2) | async-done | bytes 1310752 | tf_op jit(solution)/shard_map/all_to_all | solution.py:579
  337.4 1.1 copy-done.6
  338.5 5.9 %combine.1 = bf16[128,2048]{1,0:T(8,128)(2,1)} custom-call(bf16[2,640,512]{2,1,0:T(8,128)(2,1)} %bitcast.187, bf16[2,640,512]{2,1,0:T(8,128)(2,1)} %bitcast.186, bf16[4,256,1280]{2,1,0:T(8,128)(2,1)} %pad_maximum_fusion.refs_2_, f32[128,2048]{1,0:T(8,128)} %get-tuple-element.46.refs_3_), custom_call_target="tpu_custom_call" | custom-call | tf_op jit(solution)/shard_map/combine/pallas_call | solution.py:442
  (103 shorter events, 14.0 us)
Async XLA Ops:
  0.0 9.4 %copy-start.9 = (bf16[1024,128]{1,0:T(8,128)(2,1)S(1)}, bf16[1024,128]{1,0:T(8,128)(2,1)}, u32[]{:S(2)}) copy-start(bf16[1024,128]{1,0:T(8,128)(2,1)} %param.13) | copy-start | bytes 786436
  0.0 12.0 %copy-start.10 = (s32[128,2]{0,1:T(2,128)S(1)}, s32[128,2]{0,1:T(2,128)}, u32[]{:S(2)}) copy-start(s32[128,2]{0,1:T(2,128)} %param.21) | copy-start | bytes 3076
  3.0 10.7 %collective-permute-start.7 = (bf16[512,256]{1,0:T(8,128)(2,1)S(1)}, bf16[512,256]{1,0:T(8,128)(2,1)S(1)}, u32[]{:S(2)}, u32[]{:S(2)}) collective-permute-start(bf16[512,256]{1,0:T(8,128)(2,1)S(1)} %get-tuple-element.59), channel_id=1, source_target_pairs={{0,32},{8,40},{16,48},{24,56},{32,64},{40,72},{48,80},{56,88},{64,... | collective-permute-start | bytes 786440 | tf_op jit(solution)/shard_map/ppermute | solution.py:199
  4.6 9.1 %collective-permute-start.8 = (bf16[512,256]{1,0:T(8,128)(2,1)S(1)}, bf16[512,256]{1,0:T(8,128)(2,1)S(1)}, u32[]{:S(2)}, u32[]{:S(2)}) collective-permute-start(bf16[512,256]{1,0:T(8,128)(2,1)S(1)} %get-tuple-element.59), channel_id=1, source_target_pairs={{0,96},{8,104},{16,112},{24,120},{32,0},{40,8},{48,16},{56,24},{64... | collective-permute-start | bytes 786440 | tf_op jit(solution)/shard_map/ppermute | solution.py:199
  6.7 18.8 %collective-permute-start.3 = (bf16[512,256]{1,0:T(8,128)(2,1)S(1)}, bf16[512,256]{1,0:T(8,128)(2,1)S(1)}, u32[]{:S(2)}, u32[]{:S(2)}) collective-permute-start(bf16[512,256]{1,0:T(8,128)(2,1)S(1)} %get-tuple-element.62), channel_id=1, source_target_pairs={{0,8},{8,16},{16,24},{24,0},{32,40},{40,48},{48,56},{56,32},{64,72... | collective-permute-start | bytes 786440 | tf_op jit(solution)/shard_map/ppermute | solution.py:199
  7.9 17.7 %collective-permute-start.4 = (bf16[512,256]{1,0:T(8,128)(2,1)S(1)}, bf16[512,256]{1,0:T(8,128)(2,1)S(1)}, u32[]{:S(2)}, u32[]{:S(2)}) collective-permute-start(bf16[512,256]{1,0:T(8,128)(2,1)S(1)} %get-tuple-element.62), channel_id=1, source_target_pairs={{0,24},{8,0},{16,8},{24,16},{32,56},{40,32},{48,40},{56,48},{64,88... | collective-permute-start | bytes 786440 | tf_op jit(solution)/shard_map/ppermute | solution.py:199
  9.4 46.4 %copy-start.12 = (pred[128]{0:T(512)(128)(4,1)S(1)}, pred[128]{0:T(512)(128)(4,1)}, u32[]{:S(2)}) copy-start(pred[128]{0:T(512)(128)(4,1)} %constant.145.clone.1) | copy-start | bytes 388
  9.4 43.7 %collective-permute-start.2 = (bf16[512,128]{1,0:T(8,128)(2,1)S(1)}, bf16[512,128]{1,0:T(8,128)(2,1)S(1)}, u32[]{:S(2)}, u32[]{:S(2)}) collective-permute-start(bf16[512,128]{1,0:T(8,128)(2,1)S(1)} %bitcast.203), channel_id=1, source_target_pairs={{0,120},{8,112},{16,104},{24,96},{32,88},{40,80},{48,72},{56,64},{... | collective-permute-start | bytes 393224 | tf_op jit(solution)/shard_map/ppermute | solution.py:221
  13.6 7.8 %collective-permute-start.9 = (bf16[256,256]{1,0:T(8,128)(2,1)S(1)}, bf16[256,256]{1,0:T(8,128)(2,1)S(1)}, u32[]{:S(2)}, u32[]{:S(2)}) collective-permute-start(bf16[256,256]{1,0:T(8,128)(2,1)S(1)} %slice.90), channel_id=1, source_target_pairs={{0,32},{8,40},{16,48},{24,56},{32,64},{40,72},{48,80},{56,88},{64,... | collective-permute-start | bytes 393224 | tf_op jit(solution)/shard_map/ppermute | solution.py:200
  13.7 8.4 %collective-permute-start.10 = (bf16[256,256]{1,0:T(8,128)(2,1)S(1)}, bf16[256,256]{1,0:T(8,128)(2,1)S(1)}, u32[]{:S(2)}, u32[]{:S(2)}) collective-permute-start(bf16[256,256]{1,0:T(8,128)(2,1)S(1)} %slice.91), channel_id=1, source_target_pairs={{0,96},{8,104},{16,112},{24,120},{32,0},{40,8},{48,16},{56,24},{64... | collective-permute-start | bytes 393224 | tf_op jit(solution)/shard_map/ppermute | solution.py:200
  22.8 33.2 %collective-permute-start.16 = (bf16[2048,256]{1,0:T(8,128)(2,1)}, bf16[2048,256]{1,0:T(8,128)(2,1)S(1)}, u32[]{:S(2)}, u32[]{:S(2)}) collective-permute-start(bf16[2048,256]{1,0:T(8,128)(2,1)} %constant_dynamic-update-slice_fusion.7.refs_5_), channel_id=1, source_target_pairs={{0,8},{8,16},{16,24},{24,0},{32,40},{40,48},{48,56},{56,32},{64,72... | collective-permute-start | bytes 3145736 | tf_op jit(solution)/shard_map/ppermute | solution.py:199
  22.8 34.0 %collective-permute-start.18 = (bf16[2048,256]{1,0:T(8,128)(2,1)}, bf16[2048,256]{1,0:T(8,128)(2,1)S(1)}, u32[]{:S(2)}, u32[]{:S(2)}) collective-permute-start(bf16[2048,256]{1,0:T(8,128)(2,1)} %constant_dynamic-update-slice_fusion.7.refs_5_), channel_id=1, source_target_pairs={{0,24},{8,0},{16,8},{24,16},{32,56},{40,32},{48,40},{56,48},{64,88... | collective-permute-start | bytes 3145736 | tf_op jit(solution)/shard_map/ppermute | solution.py:199
  25.5 25.0 %collective-permute-start.5 = (bf16[256,256]{1,0:T(8,128)(2,1)S(1)}, bf16[256,256]{1,0:T(8,128)(2,1)S(1)}, u32[]{:S(2)}, u32[]{:S(2)}) collective-permute-start(bf16[256,256]{1,0:T(8,128)(2,1)S(1)} %slice.87), channel_id=1, source_target_pairs={{0,8},{8,16},{16,24},{24,0},{32,40},{40,48},{48,56},{56,32},{64,72... | collective-permute-start | bytes 393224 | tf_op jit(solution)/shard_map/ppermute | solution.py:200
  25.6 26.8 %collective-permute-start.6 = (bf16[256,256]{1,0:T(8,128)(2,1)S(1)}, bf16[256,256]{1,0:T(8,128)(2,1)S(1)}, u32[]{:S(2)}, u32[]{:S(2)}) collective-permute-start(bf16[256,256]{1,0:T(8,128)(2,1)S(1)} %slice.88), channel_id=1, source_target_pairs={{0,24},{8,0},{16,8},{24,16},{32,56},{40,32},{48,40},{56,48},{64,88... | collective-permute-start | bytes 393224 | tf_op jit(solution)/shard_map/ppermute | solution.py:200
  29.1 31.3 %copy-start = (f32[128]{0:T(128)S(1)}, f32[128]{0:T(128)}, u32[]{:S(2)}) copy-start(f32[128]{0:T(128)} %param.17) | copy-start | bytes 1540
  50.5 162.4 %collective-permute-start = (bf16[2048,640]{1,0:T(8,128)(2,1)}, bf16[2048,640]{1,0:T(8,128)(2,1)}, u32[]{:S(2)}, u32[]{:S(2)}) collective-permute-start(bf16[2048,640]{1,0:T(8,128)(2,1)} %bitcast.refs_3_), channel_id=1, source_target_pairs={{0,6},{1,3},{2,0},{3,5},{4,2},{5,7},{6,4},{7,1},{8,14},{9,11},{10,... | collective-permute-start | bytes 7864328 | tf_op jit(solution)/shard_map/ppermute | solution.py:490
  53.1 99.6 %collective-permute-start.12 = (bf16[2048,256]{1,0:T(8,128)(2,1)}, bf16[2048,256]{1,0:T(8,128)(2,1)}, u32[]{:S(2)}, u32[]{:S(2)}) collective-permute-start(bf16[2048,256]{1,0:T(8,128)(2,1)} %constant_dynamic-update-slice_fusion.2.refs_4_), channel_id=1, source_target_pairs={{0,32},{8,40},{16,48},{24,56},{32,64},{40,72},{48,80},{56,88},{64,... | collective-permute-start | bytes 3145736 | tf_op jit(solution)/shard_map/ppermute | solution.py:199
  53.1 101.8 %collective-permute-start.14 = (bf16[2048,256]{1,0:T(8,128)(2,1)}, bf16[2048,256]{1,0:T(8,128)(2,1)}, u32[]{:S(2)}, u32[]{:S(2)}) collective-permute-start(bf16[2048,256]{1,0:T(8,128)(2,1)} %constant_dynamic-update-slice_fusion.2.refs_4_), channel_id=1, source_target_pairs={{0,96},{8,104},{16,112},{24,120},{32,0},{40,8},{48,16},{56,24},{64... | collective-permute-start | bytes 3145736 | tf_op jit(solution)/shard_map/ppermute | solution.py:199
  56.8 103.6 %collective-permute-start.17 = (bf16[1024,256]{1,0:T(8,128)(2,1)}, bf16[1024,256]{1,0:T(8,128)(2,1)S(1)}, u32[]{:S(2)}, u32[]{:S(2)}) collective-permute-start(bf16[1024,256]{1,0:T(8,128)(2,1)} %slice.94), channel_id=1, source_target_pairs={{0,8},{8,16},{16,24},{24,0},{32,40},{40,48},{48,56},{56,32},{64,72... | collective-permute-start | bytes 1572872 | tf_op jit(solution)/shard_map/ppermute | solution.py:200
  57.7 102.9 %collective-permute-start.19 = (bf16[1024,256]{1,0:T(8,128)(2,1)}, bf16[1024,256]{1,0:T(8,128)(2,1)}, u32[]{:S(2)}, u32[]{:S(2)}) collective-permute-start(bf16[1024,256]{1,0:T(8,128)(2,1)} %slice.95), channel_id=1, source_target_pairs={{0,24},{8,0},{16,8},{24,16},{32,56},{40,32},{48,40},{56,48},{64,88... | collective-permute-start | bytes 1572872 | tf_op jit(solution)/shard_map/ppermute | solution.py:200
  69.8 1.4 copy-start.1
  71.2 1.0 copy-start.3
  152.8 60.9 %collective-permute-start.1 = (bf16[2048,640]{1,0:T(8,128)(2,1)}, bf16[2048,640]{1,0:T(8,128)(2,1)}, u32[]{:S(2)}, u32[]{:S(2)}) collective-permute-start(bf16[2048,640]{1,0:T(8,128)(2,1)} %bitcast.1.refs_4_), channel_id=1, source_target_pairs={{0,6},{1,3},{2,0},{3,5},{4,2},{5,7},{6,4},{7,1},{8,14},{9,11},{10,... | collective-permute-start | bytes 7864328 | tf_op jit(solution)/shard_map/ppermute | solution.py:490
  154.9 60.5 %collective-permute-start.22 = (bf16[640,2048]{1,0:T(8,128)(2,1)}, bf16[640,2048]{1,0:T(8,128)(2,1)}, u32[]{:S(2)}, u32[]{:S(2)}) collective-permute-start(bf16[640,2048]{1,0:T(8,128)(2,1)} %bitcast.189), channel_id=1, source_target_pairs={{0,1},{1,0},{2,3},{3,2},{4,5},{5,4},{6,7},{7,6},{8,9},{9,8},{10,11... | collective-permute-start | bytes 7864328 | tf_op jit(solution)/shard_map/ppermute | solution.py:495
  160.5 19.5 %collective-permute-start.13 = (bf16[1024,256]{1,0:T(8,128)(2,1)S(1)}, bf16[1024,256]{1,0:T(8,128)(2,1)S(1)}, u32[]{:S(2)}, u32[]{:S(2)}) collective-permute-start(bf16[1024,256]{1,0:T(8,128)(2,1)S(1)} %slice.92), channel_id=1, source_target_pairs={{0,32},{8,40},{16,48},{24,56},{32,64},{40,72},{48,80},{56,88},{64,... | collective-permute-start | bytes 1572872 | tf_op jit(solution)/shard_map/ppermute | solution.py:200
  160.6 19.5 %collective-permute-start.15 = (bf16[1024,256]{1,0:T(8,128)(2,1)S(1)}, bf16[1024,256]{1,0:T(8,128)(2,1)S(1)}, u32[]{:S(2)}, u32[]{:S(2)}) collective-permute-start(bf16[1024,256]{1,0:T(8,128)(2,1)S(1)} %slice.93), channel_id=1, source_target_pairs={{0,96},{8,104},{16,112},{24,120},{32,0},{40,8},{48,16},{56,24},{64... | collective-permute-start | bytes 1572872 | tf_op jit(solution)/shard_map/ppermute | solution.py:200
  163.2 1.6 copy-start.2
  164.8 1.2 copy-start.4
  180.0 32.9 %collective-permute-start.11 = (bf16[320,2048]{1,0:T(8,128)(2,1)}, bf16[320,2048]{1,0:T(8,128)(2,1)}, u32[]{:S(2)}, u32[]{:S(2)}) collective-permute-start(bf16[320,2048]{1,0:T(8,128)(2,1)} %get-tuple-element.29), channel_id=1, source_target_pairs={{0,6},{1,3},{2,0},{3,5},{4,2},{5,7},{6,4},{7,1},{8,14},{9,11},{10,... | collective-permute-start | bytes 3932168 | tf_op jit(solution)/shard_map/ppermute | solution.py:494
  180.1 35.4 %collective-permute-start.20 = (bf16[2048,640]{1,0:T(8,128)(2,1)}, bf16[2048,640]{1,0:T(8,128)(2,1)}, u32[]{:S(2)}, u32[]{:S(2)}) collective-permute-start(bf16[2048,640]{1,0:T(8,128)(2,1)} %bitcast.refs_3_), channel_id=1, source_target_pairs={{0,1},{1,0},{2,3},{3,2},{4,5},{5,4},{6,7},{7,6},{8,9},{9,8},{10,11... | collective-permute-start | bytes 7864328 | tf_op jit(solution)/shard_map/ppermute | solution.py:495
  189.6 16.7 %all-to-all-start = ((bf16[16,64,128]{2,1,0:T(8,128)(2,1)}), bf16[16,64,128]{2,1,0:T(8,128)(2,1)S(1)}, u32[]{:S(2)}, u32[]{:S(2)}) async-start(bf16[16,64,128]{2,1,0:T(8,128)(2,1)} %bitcast.12), calls=%async_computation | async-start | bytes 524288 | tf_op jit(solution)/shard_map/all_to_all | solution.py:552
  207.0 5.9 %copy-start.13 = (bf16[320,2048]{1,0:T(8,128)(2,1)S(1)}, bf16[320,2048]{1,0:T(8,128)(2,1)}, u32[]{:S(2)}) copy-start(bf16[320,2048]{1,0:T(8,128)(2,1)} %get-tuple-element.44) | copy-start | bytes 3932164
  212.9 50.8 %collective-permute-start.21 = (bf16[2048,640]{1,0:T(8,128)(2,1)}, bf16[2048,640]{1,0:T(8,128)(2,1)}, u32[]{:S(2)}, u32[]{:S(2)}) collective-permute-start(bf16[2048,640]{1,0:T(8,128)(2,1)} %bitcast.1.refs_4_), channel_id=1, source_target_pairs={{0,1},{1,0},{2,3},{3,2},{4,5},{5,4},{6,7},{7,6},{8,9},{9,8},{10,11... | collective-permute-start | bytes 7864328 | tf_op jit(solution)/shard_map/ppermute | solution.py:495
  212.9 17.6 %collective-permute-start.23 = (bf16[320,2048]{1,0:T(8,128)(2,1)S(1)}, bf16[320,2048]{1,0:T(8,128)(2,1)}, u32[]{:S(2)}, u32[]{:S(2)}) collective-permute-start(bf16[320,2048]{1,0:T(8,128)(2,1)S(1)} %copy-done.13), channel_id=1, source_target_pairs={{0,6},{1,3},{2,0},{3,5},{4,2},{5,7},{6,4},{7,1},{8,14},{9,11},{10,... | collective-permute-start | bytes 3932168 | tf_op jit(solution)/shard_map/ppermute | solution.py:558
  213.6 50.1 %collective-permute-start.24 = (bf16[2048,640]{1,0:T(8,128)(2,1)}, bf16[2048,640]{1,0:T(8,128)(2,1)}, u32[]{:S(2)}, u32[]{:S(2)}) collective-permute-start(bf16[2048,640]{1,0:T(8,128)(2,1)} %collective-permute-done.refs_9_), channel_id=1, source_target_pairs={{0,1},{1,0},{2,3},{3,2},{4,5},{5,4},{6,7},{7,6},{8,9},{9,8},{10,11... | collective-permute-start | bytes 7864328 | tf_op jit(solution)/shard_map/ppermute | solution.py:562
  215.4 48.3 %collective-permute-start.25 = (bf16[2048,640]{1,0:T(8,128)(2,1)}, bf16[2048,640]{1,0:T(8,128)(2,1)}, u32[]{:S(2)}, u32[]{:S(2)}) collective-permute-start(bf16[2048,640]{1,0:T(8,128)(2,1)} %collective-permute-done.1.refs_10_), channel_id=1, source_target_pairs={{0,1},{1,0},{2,3},{3,2},{4,5},{5,4},{6,7},{7,6},{8,9},{9,8},{10,11... | collective-permute-start | bytes 7864328 | tf_op jit(solution)/shard_map/ppermute | solution.py:562
  215.5 48.2 %collective-permute-start.26 = (bf16[320,2048]{1,0:T(8,128)(2,1)}, bf16[320,2048]{1,0:T(8,128)(2,1)}, u32[]{:S(2)}, u32[]{:S(2)}) collective-permute-start(bf16[320,2048]{1,0:T(8,128)(2,1)} %collective-permute-done.11.refs_11_), channel_id=1, source_target_pairs={{0,1},{1,0},{2,3},{3,2},{4,5},{5,4},{6,7},{7,6},{8,9},{9,8},{10,11... | collective-permute-start | bytes 3932168 | tf_op jit(solution)/shard_map/ppermute | solution.py:562
  230.4 33.3 %collective-permute-start.27 = (bf16[320,2048]{1,0:T(8,128)(2,1)}, bf16[320,2048]{1,0:T(8,128)(2,1)}, u32[]{:S(2)}, u32[]{:S(2)}) collective-permute-start(bf16[320,2048]{1,0:T(8,128)(2,1)} %collective-permute-done.23.refs_12_), channel_id=1, source_target_pairs={{0,1},{1,0},{2,3},{3,2},{4,5},{5,4},{6,7},{7,6},{8,9},{9,8},{10,11... | collective-permute-start | bytes 3932168 | tf_op jit(solution)/shard_map/ppermute | solution.py:563
  231.1 27.7 %all-to-all-start.3 = ((bf16[32,40,512]{2,1,0:T(8,128)(2,1)}), bf16[32,40,512]{2,1,0:T(8,128)(2,1)S(1)}, u32[]{:S(2)}, u32[]{:S(2)}) async-start(bf16[32,40,512]{2,1,0:T(8,128)(2,1)} %bitcast.192), calls=%async_computation.3 | async-start | bytes 2621440 | tf_op jit(solution)/shard_map/all_to_all | solution.py:579
  258.8 5.0 %copy-start.7 = (bf16[32,40,512]{2,1,0:T(8,128)(2,1)}, bf16[32,40,512]{2,1,0:T(8,128)(2,1)S(1)}, u32[]{:S(2)}) copy-start(bf16[32,40,512]{2,1,0:T(8,128)(2,1)S(1)} %all-to-all-done.3) | copy-start | bytes 3932164
  258.8 24.5 %all-to-all-start.1 = ((bf16[32,40,512]{2,1,0:T(8,128)(2,1)}), bf16[32,40,512]{2,1,0:T(8,128)(2,1)S(1)}, u32[]{:S(2)}, u32[]{:S(2)}) async-start(bf16[32,40,512]{2,1,0:T(8,128)(2,1)} %bitcast.33), calls=%async_computation.1 | async-start | bytes 2621440 | tf_op jit(solution)/shard_map/all_to_all | solution.py:579
  283.3 8.2 %copy-start.8 = (bf16[32,40,512]{2,1,0:T(8,128)(2,1)}, bf16[32,40,512]{2,1,0:T(8,128)(2,1)S(1)}, u32[]{:S(2)}) copy-start(bf16[32,40,512]{2,1,0:T(8,128)(2,1)S(1)} %all-to-all-done.1) | copy-start | bytes 3932164
  283.3 27.0 %all-to-all-start.4 = ((bf16[32,40,512]{2,1,0:T(8,128)(2,1)}), bf16[32,40,512]{2,1,0:T(8,128)(2,1)S(1)}, u32[]{:S(2)}, u32[]{:S(2)}) async-start(bf16[32,40,512]{2,1,0:T(8,128)(2,1)} %bitcast.196), calls=%async_computation.4 | async-start | bytes 2621440 | tf_op jit(solution)/shard_map/all_to_all | solution.py:579
  309.8 9.4 %copy-start.11 = (f32[128,2]{0,1:T(2,128)S(1)}, f32[128,2]{0,1:T(2,128)}, u32[]{:S(2)}) copy-start(f32[128,2]{0,1:T(2,128)} %param.22) | copy-start | bytes 3076
  310.3 9.9 %copy-start.5 = (bf16[32,40,512]{2,1,0:T(8,128)(2,1)}, bf16[32,40,512]{2,1,0:T(8,128)(2,1)S(1)}, u32[]{:S(2)}) copy-start(bf16[32,40,512]{2,1,0:T(8,128)(2,1)S(1)} %all-to-all-done.4) | copy-start | bytes 3932164
  310.3 27.1 %all-to-all-start.2 = ((bf16[32,40,512]{2,1,0:T(8,128)(2,1)}), bf16[32,40,512]{2,1,0:T(8,128)(2,1)S(1)}, u32[]{:S(2)}, u32[]{:S(2)}) async-start(bf16[32,40,512]{2,1,0:T(8,128)(2,1)} %bitcast.193), calls=%async_computation.2 | async-start | bytes 2621440 | tf_op jit(solution)/shard_map/all_to_all | solution.py:579
  337.4 1.1 copy-start.6

commit v3 on v0

--- a/solution.py
+++ b/solution.py
@@ -15,7 +15,7 @@
 BOTH = ("sp", "tp")
 F32 = jnp.float32
 BF16 = jnp.bfloat16
-VMEM_LIMIT = 58 * 1024 * 1024
+VMEM_LIMIT = 56 * 1024 * 1024
 ATTENTION_LIMIT = 26 * 1024 * 1024
 CHUNKS = 2
 CUTS = 4
@@ -276,7 +276,7 @@
     return pl.pallas_call(
         project_body,
         out_shape=(jax.ShapeDtypeStruct((rows, width), F32),) + (packed,) * CHUNKS,
-        compiler_params=pltpu.CompilerParams(vmem_limit_bytes=VMEM_LIMIT),
+        compiler_params=pltpu.CompilerParams(vmem_limit_bytes=ATTENTION_LIMIT),
         cost_estimate=cost(5),
         name="project",
     )(heads, out_weight, stream, gain.reshape(1, width), dispatch)
@@ -413,7 +413,7 @@
         combine_body,
         out_shape=jax.ShapeDtypeStruct(attended.shape, BF16),
         scratch_shapes=[pltpu.VMEM((weights.shape[2], attended.shape[1] // CUTS), BF16)],
-        compiler_params=pltpu.CompilerParams(vmem_limit_bytes=VMEM_LIMIT),
+        compiler_params=pltpu.CompilerParams(vmem_limit_bytes=ATTENTION_LIMIT),
         name="combine",
     )(*returned, weights, attended)
 

time: 253 us -> 253 us (level)
  local copies, waits for them, and re-layouts: 10.4 us -> 15.1 us
  Pallas kernels: 80 us -> 75.9 us
  other arithmetic: 10.2 us -> 6.99 us
    unnamed x38 -> x48, local copies, waits for them, and re-layouts: 6.65 us -> 11.3 us
    pallas_call x1, Pallas kernels: 5.72 us -> 3.09 us  [project(): pl.pallas_call(project_body, out_shape=(jax.ShapeDtypeStruct((rows, width...]
  transfers between devices with their start and end apart: 31 -> 31, of which waited for: 7 -> 7; matrix products, arithmetic and copies ran while one was open for 7% -> 5% of each run, Pallas kernels for 30% -> 29%
where the time goes in v3:
time: 253 us; the launch traced here: 249 us
  waiting for transfers between devices  80.1 us (32%)
  Pallas kernels  75.9 us (30%)
  starting transfers between devices  69.9 us (28%)
  local copies, waits for them, and re-layouts  15.1 us (6%)
  other arithmetic  6.99 us (3%)
    all_to_all x4, waiting for transfers between devices, exchange(): lax.all_to_all(x, BOTH, split_axis=0, concat_axis=0, tiled=True, axis_ind...  37.2 us
    pallas_call x2, Pallas kernels, expert(): pl.pallas_call(lambda *refs: expert_body(len(sets), *refs), in_specs=[pl....  36.1 us
    pallas_call x3, Pallas kernels, attention(): pl.pallas_call(lambda *refs: attention_body(pieces, side, first, final, l...  32.2 us
    all_to_all x4, starting transfers between devices, exchange(): lax.all_to_all(x, BOTH, split_axis=0, concat_axis=0, tiled=True, axis_ind...  28.2 us
    all_to_all x1, waiting for transfers between devices, local(): lax.all_to_all(heads, BOTH, split_axis=0, concat_axis=0, tiled=True, axis...  25.7 us
    ppermute x4, waiting for transfers between devices, spread(): lax.ppermute(array, 'sp', forth)  16.1 us
    unnamed x48, local copies, waits for them, and re-layouts  11.3 us
    all_to_all x1, starting transfers between devices, local(): lax.all_to_all(heads, BOTH, split_axis=0, concat_axis=0, tiled=True, axis...  9.34 us
  transfers between devices with their start and end apart: 31, of which 7 were waited for; matrix products, arithmetic and copies ran while one was open for 5% of the time, Pallas kernels for 29%

profile of v3, /device:TPU:9, one launch (start us, length us, event | category | flops | bytes accessed | tf_op | source)
XLA Modules:
  0.0 249.3 jit_solution(10912285311541730767)
XLA Ops:
  0.0 1.0 constant_dynamic-update-slice_fusion.1
  1.0 1.0 constant_dynamic-update-slice_fusion
  2.1 0.9 fusion.32
  2.9 1.6 collective-permute-start.12
  4.6 2.1 collective-permute-start.13
  6.7 1.2 collective-permute-start.4
  7.9 1.5 collective-permute-start.5
  9.4 2.5 %collective-permute-start.3 = (bf16[512,128]{1,0:T(8,128)(2,1)S(1)}, bf16[512,128]{1,0:T(8,128)(2,1)S(1)}, u32[]{:S(2)}, u32[]{:S(2)}) collective-permute-start(bf16[512,128]{1,0:T(8,128)(2,1)S(1)} %bitcast.198), channel_id=1, source_target_pairs={{0,120},{8,112},{16,104},{24,96},{32,88},{40,80},{48,72},{56,64},{... | collective-permute-start | bytes 393224 | tf_op jit(solution)/shard_map/ppermute | solution.py:221
  13.4 1.4 collective-permute-start
  14.8 0.7 constant_dynamic-update-slice_fusion.10
  15.7 0.7 constant_dynamic-update-slice_fusion.9
  16.4 2.7 %collective-permute-start.15 = (bf16[256,256]{1,0:T(8,128)(2,1)S(1)}, bf16[256,256]{1,0:T(8,128)(2,1)S(1)}, u32[]{:S(2)}, u32[]{:S(2)}) collective-permute-start(bf16[256,256]{1,0:T(8,128)(2,1)S(1)} %slice.93), channel_id=1, source_target_pairs={{0,96},{8,104},{16,112},{24,120},{32,0},{40,8},{48,16},{56,24},{64... | collective-permute-start | bytes 393224 | tf_op jit(solution)/shard_map/ppermute | solution.py:200
  19.1 0.7 constant_dynamic-update-slice_fusion.5
  20.3 0.7 constant_dynamic-update-slice_fusion.4
  21.0 1.0 collective-permute-done.14
  22.0 3.1 %collective-permute-start.7 = (bf16[256,256]{1,0:T(8,128)(2,1)S(1)}, bf16[256,256]{1,0:T(8,128)(2,1)S(1)}, u32[]{:S(2)}, u32[]{:S(2)}) collective-permute-start(bf16[256,256]{1,0:T(8,128)(2,1)S(1)} %slice.88), channel_id=1, source_target_pairs={{0,24},{8,0},{16,8},{24,16},{32,56},{40,32},{48,40},{56,48},{64,88... | collective-permute-start | bytes 393224 | tf_op jit(solution)/shard_map/ppermute | solution.py:200
  26.4 2.7 %collective-permute-start.18 = (bf16[2048,256]{1,0:T(8,128)(2,1)}, bf16[2048,256]{1,0:T(8,128)(2,1)S(1)}, u32[]{:S(2)}, u32[]{:S(2)}) collective-permute-start(bf16[2048,256]{1,0:T(8,128)(2,1)} %constant_dynamic-update-slice_fusion.7.refs_5_), channel_id=1, source_target_pairs={{0,24},{8,0},{16,8},{24,16},{32,56},{40,32},{48,40},{56,48},{64,88... | collective-permute-start | bytes 3145736 | tf_op jit(solution)/shard_map/ppermute | solution.py:199
  32.3 0.7 pad_add_fusion.1
  33.0 1.5 collective-permute-start.8
  34.6 0.7 maximum_select_fusion
  35.4 16.1 %collective-permute-done.16.refs_6_ = bf16[2048,256]{1,0:T(8,128)(2,1)S(1)} collective-permute-done((bf16[2048,256]{1,0:T(8,128)(2,1)}, bf16[2048,256]{1,0:T(8,128)(2,1)S(1)}, u32[]{:S(2)}, u32[]{:S(2)}) %collective-permute-start.16) | collective-permute-done | bytes 1048608 | tf_op jit(solution)/shard_map/ppermute | solution.py:199
  51.7 2.7 %collective-permute-start.19 = (bf16[1024,256]{1,0:T(8,128)(2,1)S(1)}, bf16[1024,256]{1,0:T(8,128)(2,1)S(1)}, u32[]{:S(2)}, u32[]{:S(2)}) collective-permute-start(bf16[1024,256]{1,0:T(8,128)(2,1)S(1)} %slice.95), channel_id=1, source_target_pairs={{0,24},{8,0},{16,8},{24,16},{32,56},{40,32},{48,40},{56,48},{64,88... | collective-permute-start | bytes 1572872 | tf_op jit(solution)/shard_map/ppermute | solution.py:200
  54.5 0.7 collective-permute-start.11
  55.2 10.1 %attention.3 = (f32[2,2,512,128]{3,2,1,0:T(8,128)S(1)}, f32[2,2,512,256]{3,2,1,0:T(8,128)S(1)}) custom-call(s32[1]{0:T(128)} %bitcast.3.refs_0_, f32[1]{0:T(128)S(6)} %copy.72.refs_1_, f32[1,128]{1,0:T(1,128)S(1)} %bitcast.185, bf16[2,2,512,128]{3,2,1,0:T(8,128)(2,1)S(1)} %pad_maximum_fusion.1.refs_3_, ...), custom_call_target="tpu_custom_call" | custom-call | flops 8000000000 | tf_op jit(solution)/shard_map/attention/pallas_call | solution.py:183
  65.6 4.5 %collective-permute-start.20 = (bf16[2048,640]{1,0:T(8,128)(2,1)}, bf16[2048,640]{1,0:T(8,128)(2,1)}, u32[]{:S(2)}, u32[]{:S(2)}) collective-permute-start(bf16[2048,640]{1,0:T(8,128)(2,1)} %bitcast.refs_3_), channel_id=1, source_target_pairs={{0,1},{1,0},{2,3},{3,2},{4,5},{5,4},{6,7},{7,6},{8,9},{9,8},{10,11... | collective-permute-start | bytes 7864328 | tf_op jit(solution)/shard_map/ppermute | solution.py:508
  70.2 1.7 collective-permute-start.9
  71.9 14.2 %attention.4 = (f32[2,2,512,128]{3,2,1,0:T(8,128)S(1)}, f32[2,2,512,256]{3,2,1,0:T(8,128)S(1)}) custom-call(s32[1]{0:T(128)} %bitcast.3.refs_0_, f32[1]{0:T(128)S(6)} %copy.72.refs_1_, f32[1,128]{1,0:T(1,128)S(1)} %bitcast.186, bf16[2,2,512,128]{3,2,1,0:T(8,128)(2,1)S(1)} %pad_maximum_fusion.1.refs_3_, bf16[2048,256]{1,0:T(8,128)(2,1)S(1)} %collective-permute-done.8.refs_4_, ...), custom_call_target="tpu_custom_call" | custom-call | flops 16000000000 | tf_op jit(solution)/shard_map/attention/pallas_call | solution.py:183
  86.1 8.0 %attention.5 = bf16[2,512,128]{2,1,0:T(8,128)(2,1)} custom-call(s32[1]{0:T(128)} %bitcast.3.refs_0_, f32[1]{0:T(128)S(6)} %copy.72.refs_1_, f32[1,128]{1,0:T(1,128)S(1)} %bitcast.187, bf16[2,2,512,128]{3,2,1,0:T(8,128)(2,1)S(1)} %pad_maximum_fusion.1.refs_3_, bf16[1024,256]{1,0:T(8,128)(2,1)S(1)} %collective-permute-done.9.refs_4_, ...), custom_call_target="tpu_custom_call" | custom-call | flops 8000000000 | tf_op jit(solution)/shard_map/attention/pallas_call | solution.py:183
  94.1 9.3 %all-to-all-start = ((bf16[16,64,128]{2,1,0:T(8,128)(2,1)}), bf16[16,64,128]{2,1,0:T(8,128)(2,1)S(1)}, u32[]{:S(2)}, u32[]{:S(2)}) async-start(bf16[16,64,128]{2,1,0:T(8,128)(2,1)} %bitcast.12), calls=%async_computation | async-start | bytes 524288 | tf_op jit(solution)/shard_map/all_to_all | solution.py:516
  103.4 0.8 fusion.6.d_ref
  104.7 25.7 %all-to-all-done = bf16[16,64,128]{2,1,0:T(8,128)(2,1)S(1)} async-done(((bf16[16,64,128]{2,1,0:T(8,128)(2,1)}), bf16[16,64,128]{2,1,0:T(8,128)(2,1)S(1)}, u32[]{:S(2)}, u32[]{:S(2)}) %all-to-all-start) | async-done | bytes 262176 | tf_op jit(solution)/shard_map/all_to_all | solution.py:516
  130.5 2.2 copy-done.4
  132.7 3.1 %project.1 = (f32[128,2048]{1,0:T(8,128)S(1)}, bf16[2,640,512]{2,1,0:T(8,128)(2,1)}, bf16[2,640,512]{2,1,0:T(8,128)(2,1)}) custom-call(bf16[2,8,64,128]{3,2,1,0:T(8,128)(2,1)S(1)} %reverse_select_fusion.h_ref, bf16[1024,2048]{1,0:T(8,128)(2,1)S(1)} %copy-done.4, bf16[128,2048]{1,0:T(8,128)(2,1)S(1)} %copy-done.5, f32[1,2048]{1,0:T(1,128)S(1)} %bitcast.184, ...), custom_call_target="tpu_custom_call" | custom-call | flops 5000000000 | tf_op jit(solution)/shard_map/project/pallas_call | solution.py:276
  135.7 1.0 copy-done.2
  137.8 6.1 %all-to-all-start.3 = ((bf16[32,40,512]{2,1,0:T(8,128)(2,1)}), bf16[32,40,512]{2,1,0:T(8,128)(2,1)S(1)}, u32[]{:S(2)}, u32[]{:S(2)}) async-start(bf16[32,40,512]{2,1,0:T(8,128)(2,1)} %bitcast.37), calls=%async_computation.3 | async-start | bytes 2621440 | tf_op jit(solution)/shard_map/all_to_all | solution.py:540
  144.0 1.4 fusion.5
  145.5 18.5 %all-to-all-done.3 = bf16[32,40,512]{2,1,0:T(8,128)(2,1)S(1)} async-done(((bf16[32,40,512]{2,1,0:T(8,128)(2,1)}), bf16[32,40,512]{2,1,0:T(8,128)(2,1)S(1)}, u32[]{:S(2)}, u32[]{:S(2)}) %all-to-all-start.3) | async-done | bytes 1310752 | tf_op jit(solution)/shard_map/all_to_all | solution.py:540
  164.0 5.4 %all-to-all-start.1 = ((bf16[32,40,512]{2,1,0:T(8,128)(2,1)}), bf16[32,40,512]{2,1,0:T(8,128)(2,1)S(1)}, u32[]{:S(2)}, u32[]{:S(2)}) async-start(bf16[32,40,512]{2,1,0:T(8,128)(2,1)} %bitcast.33), calls=%async_computation.1 | async-start | bytes 2621440 | tf_op jit(solution)/shard_map/all_to_all | solution.py:540
  169.4 18.0 %expert.3 = bf16[2,640,512]{2,1,0:T(8,128)(2,1)} custom-call(bf16[2,640,512]{2,1,0:T(8,128)(2,1)} %bitcast.189, bf16[640,640]{1,0:T(8,128)(2,1)} %get-tuple-element.62.refs_1_, bf16[640,640]{1,0:T(8,128)(2,1)} %get-tuple-element.61.refs_2_, bf16[2048,640]{1,0:T(8,128)(2,1)} %bitcast.refs_3_, bf16[2048,640]{1,0:T(8,128)(2,1)} %bitcast.1.refs_4_, ...), custom_call_target="tpu_custom_call" | custom-call | flops 16000000000 | tf_op jit(solution)/shard_map/expert/pallas_call | solution.py:371
  187.5 1.3 all-to-all-done.1
  188.7 7.8 %all-to-all-start.4 = ((bf16[32,40,512]{2,1,0:T(8,128)(2,1)}), bf16[32,40,512]{2,1,0:T(8,128)(2,1)S(1)}, u32[]{:S(2)}, u32[]{:S(2)}) async-start(bf16[32,40,512]{2,1,0:T(8,128)(2,1)} %bitcast.191), calls=%async_computation.4 | async-start | bytes 2621440 | tf_op jit(solution)/shard_map/all_to_all | solution.py:540
  196.6 18.1 %expert.2 = bf16[2,640,512]{2,1,0:T(8,128)(2,1)} custom-call(bf16[2,640,512]{2,1,0:T(8,128)(2,1)} %bitcast.190, bf16[640,640]{1,0:T(8,128)(2,1)} %get-tuple-element.62.refs_1_, bf16[640,640]{1,0:T(8,128)(2,1)} %get-tuple-element.61.refs_2_, bf16[2048,640]{1,0:T(8,128)(2,1)} %bitcast.refs_3_, bf16[2048,640]{1,0:T(8,128)(2,1)} %bitcast.1.refs_4_, ...), custom_call_target="tpu_custom_call" | custom-call | flops 16000000000 | tf_op jit(solution)/shard_map/expert/pallas_call | solution.py:371
  215.3 8.9 %all-to-all-start.2 = ((bf16[32,40,512]{2,1,0:T(8,128)(2,1)}), bf16[32,40,512]{2,1,0:T(8,128)(2,1)}, u32[]{:S(2)}, u32[]{:S(2)}) async-start(bf16[32,40,512]{2,1,0:T(8,128)(2,1)} %bitcast.188), calls=%async_computation.2 | async-start | bytes 2621440 | tf_op jit(solution)/shard_map/all_to_all | solution.py:540
  224.3 1.0 fusion.1
  225.5 16.9 %all-to-all-done.2 = bf16[32,40,512]{2,1,0:T(8,128)(2,1)} async-done(((bf16[32,40,512]{2,1,0:T(8,128)(2,1)}), bf16[32,40,512]{2,1,0:T(8,128)(2,1)}, u32[]{:S(2)}, u32[]{:S(2)}) %all-to-all-start.2) | async-done | bytes 1310752 | tf_op jit(solution)/shard_map/all_to_all | solution.py:540
  242.4 1.3 copy-done.1
  243.7 1.2 copy-done.3
  244.9 4.4 %combine.1 = bf16[128,2048]{1,0:T(8,128)(2,1)} custom-call(bf16[2,640,512]{2,1,0:T(8,128)(2,1)} %bitcast.36.refs_0_, bf16[2,640,512]{2,1,0:T(8,128)(2,1)S(1)} %bitcast.183, bf16[4,256,1280]{2,1,0:T(8,128)(2,1)S(1)} %pad_maximum_fusion.refs_2_, f32[128,2048]{1,0:T(8,128)S(1)} %copy-done.3), custom_call_target="tpu_custom_call" | custom-call | tf_op jit(solution)/shard_map/combine/pallas_call | solution.py:412
  (108 shorter events, 9.2 us)
Async XLA Ops:
  0.0 9.4 %copy-start.10 = (bf16[1024,128]{1,0:T(8,128)(2,1)S(1)}, bf16[1024,128]{1,0:T(8,128)(2,1)}, u32[]{:S(2)}) copy-start(bf16[1024,128]{1,0:T(8,128)(2,1)} %param.13) | copy-start | bytes 786436
  0.0 11.9 %copy-start.11 = (s32[128,2]{0,1:T(2,128)S(1)}, s32[128,2]{0,1:T(2,128)}, u32[]{:S(2)}) copy-start(s32[128,2]{0,1:T(2,128)} %param.21) | copy-start | bytes 3076
  2.9 10.5 %collective-permute-start.12 = (bf16[512,256]{1,0:T(8,128)(2,1)S(1)}, bf16[512,256]{1,0:T(8,128)(2,1)S(1)}, u32[]{:S(2)}, u32[]{:S(2)}) collective-permute-start(bf16[512,256]{1,0:T(8,128)(2,1)S(1)} %get-tuple-element.51), channel_id=1, source_target_pairs={{0,32},{8,40},{16,48},{24,56},{32,64},{40,72},{48,80},{56,88},{64,... | collective-permute-start | bytes 786440 | tf_op jit(solution)/shard_map/ppermute | solution.py:199
  4.6 11.0 %collective-permute-start.13 = (bf16[512,256]{1,0:T(8,128)(2,1)S(1)}, bf16[512,256]{1,0:T(8,128)(2,1)S(1)}, u32[]{:S(2)}, u32[]{:S(2)}) collective-permute-start(bf16[512,256]{1,0:T(8,128)(2,1)S(1)} %get-tuple-element.51), channel_id=1, source_target_pairs={{0,96},{8,104},{16,112},{24,120},{32,0},{40,8},{48,16},{56,24},{64... | collective-permute-start | bytes 786440 | tf_op jit(solution)/shard_map/ppermute | solution.py:199
  6.7 9.7 %collective-permute-start.4 = (bf16[512,256]{1,0:T(8,128)(2,1)S(1)}, bf16[512,256]{1,0:T(8,128)(2,1)S(1)}, u32[]{:S(2)}, u32[]{:S(2)}) collective-permute-start(bf16[512,256]{1,0:T(8,128)(2,1)S(1)} %get-tuple-element.54), channel_id=1, source_target_pairs={{0,8},{8,16},{16,24},{24,0},{32,40},{40,48},{48,56},{56,32},{64,72... | collective-permute-start | bytes 786440 | tf_op jit(solution)/shard_map/ppermute | solution.py:199
  7.9 11.9 %collective-permute-start.5 = (bf16[512,256]{1,0:T(8,128)(2,1)S(1)}, bf16[512,256]{1,0:T(8,128)(2,1)S(1)}, u32[]{:S(2)}, u32[]{:S(2)}) collective-permute-start(bf16[512,256]{1,0:T(8,128)(2,1)S(1)} %get-tuple-element.54), channel_id=1, source_target_pairs={{0,24},{8,0},{16,8},{24,16},{32,56},{40,32},{48,40},{56,48},{64,88... | collective-permute-start | bytes 786440 | tf_op jit(solution)/shard_map/ppermute | solution.py:199
  9.4 23.6 %collective-permute-start.3 = (bf16[512,128]{1,0:T(8,128)(2,1)S(1)}, bf16[512,128]{1,0:T(8,128)(2,1)S(1)}, u32[]{:S(2)}, u32[]{:S(2)}) collective-permute-start(bf16[512,128]{1,0:T(8,128)(2,1)S(1)} %bitcast.198), channel_id=1, source_target_pairs={{0,120},{8,112},{16,104},{24,96},{32,88},{40,80},{48,72},{56,64},{... | collective-permute-start | bytes 393224 | tf_op jit(solution)/shard_map/ppermute | solution.py:221
  12.8 18.9 %copy-start.12 = (s32[128,1]{0,1:T(1,128)}, s32[128,1]{0,1:T(1,128)S(1)}, u32[]{:S(2)}) copy-start(s32[128,1]{0,1:T(1,128)S(1)} %copy.62) | copy-start | bytes 1540
  13.4 123.3 %collective-permute-start = (bf16[2048,640]{1,0:T(8,128)(2,1)}, bf16[2048,640]{1,0:T(8,128)(2,1)}, u32[]{:S(2)}, u32[]{:S(2)}) collective-permute-start(bf16[2048,640]{1,0:T(8,128)(2,1)} %bitcast.refs_3_), channel_id=1, source_target_pairs={{0,6},{1,3},{2,0},{3,5},{4,2},{5,7},{6,4},{7,1},{8,14},{9,11},{10,... | collective-permute-start | bytes 7864328 | tf_op jit(solution)/shard_map/ppermute | solution.py:459
  15.6 6.5 %collective-permute-start.14 = (bf16[256,256]{1,0:T(8,128)(2,1)S(1)}, bf16[256,256]{1,0:T(8,128)(2,1)S(1)}, u32[]{:S(2)}, u32[]{:S(2)}) collective-permute-start(bf16[256,256]{1,0:T(8,128)(2,1)S(1)} %slice.92), channel_id=1, source_target_pairs={{0,32},{8,40},{16,48},{24,56},{32,64},{40,72},{48,80},{56,88},{64,... | collective-permute-start | bytes 393224 | tf_op jit(solution)/shard_map/ppermute | solution.py:200
  16.4 9.4 %collective-permute-start.15 = (bf16[256,256]{1,0:T(8,128)(2,1)S(1)}, bf16[256,256]{1,0:T(8,128)(2,1)S(1)}, u32[]{:S(2)}, u32[]{:S(2)}) collective-permute-start(bf16[256,256]{1,0:T(8,128)(2,1)S(1)} %slice.93), channel_id=1, source_target_pairs={{0,96},{8,104},{16,112},{24,120},{32,0},{40,8},{48,16},{56,24},{64... | collective-permute-start | bytes 393224 | tf_op jit(solution)/shard_map/ppermute | solution.py:200
  19.8 6.7 %collective-permute-start.6 = (bf16[256,256]{1,0:T(8,128)(2,1)S(1)}, bf16[256,256]{1,0:T(8,128)(2,1)S(1)}, u32[]{:S(2)}, u32[]{:S(2)}) collective-permute-start(bf16[256,256]{1,0:T(8,128)(2,1)S(1)} %slice.87), channel_id=1, source_target_pairs={{0,8},{8,16},{16,24},{24,0},{32,40},{40,48},{48,56},{56,32},{64,72... | collective-permute-start | bytes 393224 | tf_op jit(solution)/shard_map/ppermute | solution.py:200
  22.0 7.8 %collective-permute-start.7 = (bf16[256,256]{1,0:T(8,128)(2,1)S(1)}, bf16[256,256]{1,0:T(8,128)(2,1)S(1)}, u32[]{:S(2)}, u32[]{:S(2)}) collective-permute-start(bf16[256,256]{1,0:T(8,128)(2,1)S(1)} %slice.88), channel_id=1, source_target_pairs={{0,24},{8,0},{16,8},{24,16},{32,56},{40,32},{48,40},{56,48},{64,88... | collective-permute-start | bytes 393224 | tf_op jit(solution)/shard_map/ppermute | solution.py:200
  26.4 25.1 %collective-permute-start.16 = (bf16[2048,256]{1,0:T(8,128)(2,1)}, bf16[2048,256]{1,0:T(8,128)(2,1)S(1)}, u32[]{:S(2)}, u32[]{:S(2)}) collective-permute-start(bf16[2048,256]{1,0:T(8,128)(2,1)} %constant_dynamic-update-slice_fusion.7.refs_5_), channel_id=1, source_target_pairs={{0,8},{8,16},{16,24},{24,0},{32,40},{40,48},{48,56},{56,32},{64,72... | collective-permute-start | bytes 3145736 | tf_op jit(solution)/shard_map/ppermute | solution.py:199
  26.4 25.2 %collective-permute-start.18 = (bf16[2048,256]{1,0:T(8,128)(2,1)}, bf16[2048,256]{1,0:T(8,128)(2,1)S(1)}, u32[]{:S(2)}, u32[]{:S(2)}) collective-permute-start(bf16[2048,256]{1,0:T(8,128)(2,1)} %constant_dynamic-update-slice_fusion.7.refs_5_), channel_id=1, source_target_pairs={{0,24},{8,0},{16,8},{24,16},{32,56},{40,32},{48,40},{56,48},{64,88... | collective-permute-start | bytes 3145736 | tf_op jit(solution)/shard_map/ppermute | solution.py:199
  30.5 24.0 %collective-permute-start.10 = (bf16[2048,256]{1,0:T(8,128)(2,1)}, bf16[2048,256]{1,0:T(8,128)(2,1)S(1)}, u32[]{:S(2)}, u32[]{:S(2)}) collective-permute-start(bf16[2048,256]{1,0:T(8,128)(2,1)} %constant_dynamic-update-slice_fusion.2.refs_4_), channel_id=1, source_target_pairs={{0,96},{8,104},{16,112},{24,120},{32,0},{40,8},{48,16},{56,24},{64... | collective-permute-start | bytes 3145736 | tf_op jit(solution)/shard_map/ppermute | solution.py:199
  33.0 32.3 %collective-permute-start.8 = (bf16[2048,256]{1,0:T(8,128)(2,1)}, bf16[2048,256]{1,0:T(8,128)(2,1)S(1)}, u32[]{:S(2)}, u32[]{:S(2)}) collective-permute-start(bf16[2048,256]{1,0:T(8,128)(2,1)} %constant_dynamic-update-slice_fusion.2.refs_4_), channel_id=1, source_target_pairs={{0,32},{8,40},{16,48},{24,56},{32,64},{40,72},{48,80},{56,88},{64,... | collective-permute-start | bytes 3145736 | tf_op jit(solution)/shard_map/ppermute | solution.py:199
  34.6 20.6 %copy-start.7 = (f32[128]{0:T(128)S(1)}, f32[128]{0:T(128)}, u32[]{:S(2)}) copy-start(f32[128]{0:T(128)} %param.17) | copy-start | bytes 1540
  51.6 14.0 %collective-permute-start.17 = (bf16[1024,256]{1,0:T(8,128)(2,1)S(1)}, bf16[1024,256]{1,0:T(8,128)(2,1)S(1)}, u32[]{:S(2)}, u32[]{:S(2)}) collective-permute-start(bf16[1024,256]{1,0:T(8,128)(2,1)S(1)} %slice.94), channel_id=1, source_target_pairs={{0,8},{8,16},{16,24},{24,0},{32,40},{40,48},{48,56},{56,32},{64,72... | collective-permute-start | bytes 1572872 | tf_op jit(solution)/shard_map/ppermute | solution.py:200
  51.7 13.9 %collective-permute-start.19 = (bf16[1024,256]{1,0:T(8,128)(2,1)S(1)}, bf16[1024,256]{1,0:T(8,128)(2,1)S(1)}, u32[]{:S(2)}, u32[]{:S(2)}) collective-permute-start(bf16[1024,256]{1,0:T(8,128)(2,1)S(1)} %slice.95), channel_id=1, source_target_pairs={{0,24},{8,0},{16,8},{24,16},{32,56},{40,32},{48,40},{56,48},{64,88... | collective-permute-start | bytes 1572872 | tf_op jit(solution)/shard_map/ppermute | solution.py:200
  54.5 15.7 %collective-permute-start.11 = (bf16[1024,256]{1,0:T(8,128)(2,1)S(1)}, bf16[1024,256]{1,0:T(8,128)(2,1)S(1)}, u32[]{:S(2)}, u32[]{:S(2)}) collective-permute-start(bf16[1024,256]{1,0:T(8,128)(2,1)S(1)} %slice.90), channel_id=1, source_target_pairs={{0,96},{8,104},{16,112},{24,120},{32,0},{40,8},{48,16},{56,24},{64... | collective-permute-start | bytes 1572872 | tf_op jit(solution)/shard_map/ppermute | solution.py:200
  65.3 71.8 %collective-permute-start.1 = (bf16[2048,640]{1,0:T(8,128)(2,1)}, bf16[2048,640]{1,0:T(8,128)(2,1)}, u32[]{:S(2)}, u32[]{:S(2)}) collective-permute-start(bf16[2048,640]{1,0:T(8,128)(2,1)} %bitcast.1.refs_4_), channel_id=1, source_target_pairs={{0,6},{1,3},{2,0},{3,5},{4,2},{5,7},{6,4},{7,1},{8,14},{9,11},{10,... | collective-permute-start | bytes 7864328 | tf_op jit(solution)/shard_map/ppermute | solution.py:459
  65.6 71.5 %collective-permute-start.2 = (bf16[640,2048]{1,0:T(8,128)(2,1)}, bf16[640,2048]{1,0:T(8,128)(2,1)}, u32[]{:S(2)}, u32[]{:S(2)}) collective-permute-start(bf16[640,2048]{1,0:T(8,128)(2,1)} %bitcast.2.refs_5_), channel_id=1, source_target_pairs={{0,6},{1,3},{2,0},{3,5},{4,2},{5,7},{6,4},{7,1},{8,14},{9,11},{10,... | collective-permute-start | bytes 7864328 | tf_op jit(solution)/shard_map/ppermute | solution.py:459
  65.6 72.0 %collective-permute-start.20 = (bf16[2048,640]{1,0:T(8,128)(2,1)}, bf16[2048,640]{1,0:T(8,128)(2,1)}, u32[]{:S(2)}, u32[]{:S(2)}) collective-permute-start(bf16[2048,640]{1,0:T(8,128)(2,1)} %bitcast.refs_3_), channel_id=1, source_target_pairs={{0,1},{1,0},{2,3},{3,2},{4,5},{5,4},{6,7},{7,6},{8,9},{9,8},{10,11... | collective-permute-start | bytes 7864328 | tf_op jit(solution)/shard_map/ppermute | solution.py:508
  70.2 15.9 %collective-permute-start.9 = (bf16[1024,256]{1,0:T(8,128)(2,1)S(1)}, bf16[1024,256]{1,0:T(8,128)(2,1)S(1)}, u32[]{:S(2)}, u32[]{:S(2)}) collective-permute-start(bf16[1024,256]{1,0:T(8,128)(2,1)S(1)} %slice.89), channel_id=1, source_target_pairs={{0,32},{8,40},{16,48},{24,56},{32,64},{40,72},{48,80},{56,88},{64,... | collective-permute-start | bytes 1572872 | tf_op jit(solution)/shard_map/ppermute | solution.py:200
  86.1 44.4 %copy-start.5 = (bf16[128,2048]{1,0:T(8,128)(2,1)S(1)}, bf16[128,2048]{1,0:T(8,128)(2,1)}, u32[]{:S(2)}) copy-start(bf16[128,2048]{1,0:T(8,128)(2,1)} %s_ref.1) | copy-start | bytes 1572868
  86.1 44.4 %copy-start.6 = (f32[2048]{0:T(1024)S(1)}, f32[2048]{0:T(1024)}, u32[]{:S(2)}) copy-start(f32[2048]{0:T(1024)} %param.20) | copy-start | bytes 24580
  94.1 36.3 %all-to-all-start = ((bf16[16,64,128]{2,1,0:T(8,128)(2,1)}), bf16[16,64,128]{2,1,0:T(8,128)(2,1)S(1)}, u32[]{:S(2)}, u32[]{:S(2)}) async-start(bf16[16,64,128]{2,1,0:T(8,128)(2,1)} %bitcast.12), calls=%async_computation | async-start | bytes 524288 | tf_op jit(solution)/shard_map/all_to_all | solution.py:516
  104.2 65.2 %collective-permute-start.21 = (bf16[2048,640]{1,0:T(8,128)(2,1)}, bf16[2048,640]{1,0:T(8,128)(2,1)}, u32[]{:S(2)}, u32[]{:S(2)}) collective-permute-start(bf16[2048,640]{1,0:T(8,128)(2,1)} %bitcast.1.refs_4_), channel_id=1, source_target_pairs={{0,1},{1,0},{2,3},{3,2},{4,5},{5,4},{6,7},{7,6},{8,9},{9,8},{10,11... | collective-permute-start | bytes 7864328 | tf_op jit(solution)/shard_map/ppermute | solution.py:508
  130.5 2.2 copy-start.4
  136.7 32.6 %collective-permute-start.22 = (bf16[640,2048]{1,0:T(8,128)(2,1)}, bf16[640,2048]{1,0:T(8,128)(2,1)}, u32[]{:S(2)}, u32[]{:S(2)}) collective-permute-start(bf16[640,2048]{1,0:T(8,128)(2,1)} %bitcast.2.refs_5_), channel_id=1, source_target_pairs={{0,1},{1,0},{2,3},{3,2},{4,5},{5,4},{6,7},{7,6},{8,9},{9,8},{10,11... | collective-permute-start | bytes 7864328 | tf_op jit(solution)/shard_map/ppermute | solution.py:508
  137.1 32.3 %collective-permute-start.23 = (bf16[2048,640]{1,0:T(8,128)(2,1)}, bf16[2048,640]{1,0:T(8,128)(2,1)}, u32[]{:S(2)}, u32[]{:S(2)}) collective-permute-start(bf16[2048,640]{1,0:T(8,128)(2,1)} %collective-permute-done.refs_9_), channel_id=1, source_target_pairs={{0,1},{1,0},{2,3},{3,2},{4,5},{5,4},{6,7},{7,6},{8,9},{9,8},{10,11... | collective-permute-start | bytes 7864328 | tf_op jit(solution)/shard_map/ppermute | solution.py:524
  137.3 32.2 %collective-permute-start.24 = (bf16[2048,640]{1,0:T(8,128)(2,1)}, bf16[2048,640]{1,0:T(8,128)(2,1)}, u32[]{:S(2)}, u32[]{:S(2)}) collective-permute-start(bf16[2048,640]{1,0:T(8,128)(2,1)} %collective-permute-done.1.refs_10_), channel_id=1, source_target_pairs={{0,1},{1,0},{2,3},{3,2},{4,5},{5,4},{6,7},{7,6},{8,9},{9,8},{10,11... | collective-permute-start | bytes 7864328 | tf_op jit(solution)/shard_map/ppermute | solution.py:524
  137.6 31.8 %collective-permute-start.25 = (bf16[640,2048]{1,0:T(8,128)(2,1)}, bf16[640,2048]{1,0:T(8,128)(2,1)}, u32[]{:S(2)}, u32[]{:S(2)}) collective-permute-start(bf16[640,2048]{1,0:T(8,128)(2,1)} %collective-permute-done.2.refs_11_), channel_id=1, source_target_pairs={{0,1},{1,0},{2,3},{3,2},{4,5},{5,4},{6,7},{7,6},{8,9},{9,8},{10,11... | collective-permute-start | bytes 7864328 | tf_op jit(solution)/shard_map/ppermute | solution.py:524
  137.8 26.2 %all-to-all-start.3 = ((bf16[32,40,512]{2,1,0:T(8,128)(2,1)}), bf16[32,40,512]{2,1,0:T(8,128)(2,1)S(1)}, u32[]{:S(2)}, u32[]{:S(2)}) async-start(bf16[32,40,512]{2,1,0:T(8,128)(2,1)} %bitcast.37), calls=%async_computation.3 | async-start | bytes 2621440 | tf_op jit(solution)/shard_map/all_to_all | solution.py:540
  164.0 5.5 %copy-start.8 = (bf16[32,40,512]{2,1,0:T(8,128)(2,1)}, bf16[32,40,512]{2,1,0:T(8,128)(2,1)S(1)}, u32[]{:S(2)}) copy-start(bf16[32,40,512]{2,1,0:T(8,128)(2,1)S(1)} %all-to-all-done.3) | copy-start | bytes 3932164
  164.0 24.8 %all-to-all-start.1 = ((bf16[32,40,512]{2,1,0:T(8,128)(2,1)}), bf16[32,40,512]{2,1,0:T(8,128)(2,1)S(1)}, u32[]{:S(2)}, u32[]{:S(2)}) async-start(bf16[32,40,512]{2,1,0:T(8,128)(2,1)} %bitcast.33), calls=%async_computation.1 | async-start | bytes 2621440 | tf_op jit(solution)/shard_map/all_to_all | solution.py:540
  188.7 7.8 %copy-start.9 = (bf16[32,40,512]{2,1,0:T(8,128)(2,1)}, bf16[32,40,512]{2,1,0:T(8,128)(2,1)S(1)}, u32[]{:S(2)}) copy-start(bf16[32,40,512]{2,1,0:T(8,128)(2,1)S(1)} %all-to-all-done.1) | copy-start | bytes 3932164
  188.7 26.6 %all-to-all-start.4 = ((bf16[32,40,512]{2,1,0:T(8,128)(2,1)}), bf16[32,40,512]{2,1,0:T(8,128)(2,1)S(1)}, u32[]{:S(2)}, u32[]{:S(2)}) async-start(bf16[32,40,512]{2,1,0:T(8,128)(2,1)} %bitcast.191), calls=%async_computation.4 | async-start | bytes 2621440 | tf_op jit(solution)/shard_map/all_to_all | solution.py:540
  214.7 9.5 %copy-start.13 = (s32[128,1]{0,1:T(1,128)S(1)}, s32[128,1]{0,1:T(1,128)}, u32[]{:S(2)}) copy-start(s32[128,1]{0,1:T(1,128)} %copy-done.12) | copy-start | bytes 1540
  214.7 9.5 %copy-start.16 = (s32[1,128]{1,0:T(1,128)S(1)}, s32[1,128]{1,0:T(1,128)}, u32[]{:S(2)}) copy-start(s32[1,128]{1,0:T(1,128)} %get-tuple-element.40) | copy-start | bytes 1540
  214.7 9.5 %copy-start.17 = (s32[1,128]{1,0:T(1,128)S(1)}, s32[1,128]{1,0:T(1,128)}, u32[]{:S(2)}) copy-start(s32[1,128]{1,0:T(1,128)} %get-tuple-element.99) | copy-start | bytes 1540
  214.7 9.5 %copy-start.14 = (s32[1,128]{1,0:T(1,128)S(1)}, s32[1,128]{1,0:T(1,128)}, u32[]{:S(2)}) copy-start(s32[1,128]{1,0:T(1,128)} %get-tuple-element.39) | copy-start | bytes 1540
  214.7 9.5 %copy-start.15 = (s32[1,128]{1,0:T(1,128)S(1)}, s32[1,128]{1,0:T(1,128)}, u32[]{:S(2)}) copy-start(s32[1,128]{1,0:T(1,128)} %get-tuple-element.98) | copy-start | bytes 1540
  214.8 9.5 %copy-start.18 = (f32[128,2]{0,1:T(2,128)S(1)}, f32[128,2]{0,1:T(2,128)}, u32[]{:S(2)}) copy-start(f32[128,2]{0,1:T(2,128)} %param.22) | copy-start | bytes 3076
  215.3 10.0 %copy-start = (bf16[32,40,512]{2,1,0:T(8,128)(2,1)}, bf16[32,40,512]{2,1,0:T(8,128)(2,1)S(1)}, u32[]{:S(2)}) copy-start(bf16[32,40,512]{2,1,0:T(8,128)(2,1)S(1)} %all-to-all-done.4) | copy-start | bytes 3932164
  215.3 27.1 %all-to-all-start.2 = ((bf16[32,40,512]{2,1,0:T(8,128)(2,1)}), bf16[32,40,512]{2,1,0:T(8,128)(2,1)}, u32[]{:S(2)}, u32[]{:S(2)}) async-start(bf16[32,40,512]{2,1,0:T(8,128)(2,1)} %bitcast.188), calls=%async_computation.2 | async-start | bytes 2621440 | tf_op jit(solution)/shard_map/all_to_all | solution.py:540
  242.4 1.3 copy-start.1
  (2 other events, 2.2 us)
